TPU v7x, 256 devices: a whole 4x4x8 slice. The times are simulated.
256 devices in a mesh: sp: 64 (over z, x, core), tp: 4 (over y).
Axes of the slice: x: 4, y: 4, z: 8, core: 2. Of those that a mesh axis runs over, the one named last changes fastest.
Arguments:
- residual_in: bfloat16 [16384, 2048], P('sp', 'tp'), may hold values from -6 to 6
- conv_input: bfloat16 [16384, 512], P('sp', 'tp'), may hold values from -6 to 6
- outer_gate: bfloat16 [16384, 512], P('sp', 'tp'), may hold values from -6 to 6
- inner_gate: bfloat16 [16384, 512], P('sp', 'tp'), may hold values from -6 to 6
- documents: int32 [16384], P('sp'), may hold values from 0 to 31, as said below
- conv_taps: float32 [3, 512], P(None, 'tp'), may hold values from -3 to 3
- mixer_gain: float32 [512], replicated, may hold values from 0.1 to 1.9
- output_weight: bfloat16 [512, 2048], P(None, 'tp'), may hold values from -0.25 to 0.25
- ffn_gain: float32 [2048], P('tp'), may hold values from 0.1 to 1.9
- routes: int32 [16384, 2], P('sp'), may hold values from 0 to 63, all different within a row; in each aligned block of 256 rows (0 to 255, 256 to 511, ...) at most 16 rows name the same one
- route_weights: float32 [16384, 2], P('sp'), may hold values from 0.1 to 0.9
- expert_gate: bfloat16 [64, 2048, 3584], P('sp', None, 'tp'), may hold values from -0.125 to 0.125
- expert_up: bfloat16 [64, 2048, 3584], P('sp', None, 'tp'), may hold values from -0.125 to 0.125
- expert_down: bfloat16 [64, 3584, 2048], P('sp', 'tp'), may hold values from -0.09375 to 0.09375
Outputs:
- layer_out: bfloat16 [16384, 2048], P('sp', 'tp')
Inputs may be any that keep to these rules, and one draw needn't show every extreme that they name: Document numbers never fall along the positions, and each of the 32 documents occurs. Every document has 256 to 768 positions, and one has exactly 768. `routes`: the two experts of a position differ. Among the 256 positions of one index of sp no expert is named more than 16 times, a bound that some block reaches.
All inputs are finite; a program needn't handle non-finite values.
Results may differ from a plain program's by a relative error of at most 0.0058.
Values may be sent and summed in bfloat16 or wider, within the bound.
A program may use at most 64 MiB of HBM per device.

v0:
```python
import jax
import jax.numpy as jnp
from jax import lax
from jax.sharding import PartitionSpec as P

EPS = 1e-06


def from_behind(block, axis, distance):
    devices = range(lax.axis_size(axis))
    route = [(i - distance, i) for i in devices if i - distance in devices]
    return lax.ppermute(block, axis, route)


def laid_out(pieces, dim):
    dims = list(pieces.shape[1:])
    dims[dim] *= pieces.shape[0]
    return jnp.moveaxis(pieces, 0, dim).reshape(dims)


def sent_to_all(shard, axis):
    copies = jnp.broadcast_to(shard, (lax.axis_size(axis), *shard.shape))
    return lax.all_to_all(copies, axis, split_axis=0, concat_axis=0, tiled=True)


def gather_directly(shard, axis, dim):
    return laid_out(sent_to_all(shard, axis), dim)


def over_copies(shard, axis):
    return sent_to_all(shard, axis).sum(axis=0)


def slot_tables(routes, experts, capacity):
    tokens = routes.shape[0]
    flattened = routes.reshape(-1)
    onehot = (flattened[:, None] == jnp.arange(experts, dtype=jnp.int32)[None, :]).astype(jnp.int32)
    earlier = jnp.cumsum(onehot, axis=0) - onehot
    position_in = jnp.sum(earlier * onehot, axis=1)
    target = flattened * capacity + position_in
    owners = (
        jnp.full((experts * capacity,), tokens, jnp.int32)
        .at[target]
        .set(jnp.arange(2 * tokens, dtype=jnp.int32) // 2)
    )
    return (target, owners)


def per_device(
    residual_in,
    conv_input,
    outer_gate,
    inner_gate,
    documents,
    conv_taps,
    mixer_gain,
    output_weight,
    ffn_gain,
    routes,
    route_weights,
    expert_gate,
    expert_up,
    expert_down,
):
    tokens_here = residual_in.shape[0]
    local_features = residual_in.shape[1]
    conv_value = (inner_gate.astype(jnp.float32) * conv_input.astype(jnp.float32)).astype(
        jnp.bfloat16
    )
    doc_marks = documents.astype(jnp.bfloat16)
    before_rows, before_docs = from_behind((conv_value[-2:], doc_marks[-2:]), "sp", 1)
    joined_rows = jnp.concatenate([before_rows, conv_value], axis=0).astype(jnp.float32)
    joined_docs = jnp.concatenate([before_docs, doc_marks], axis=0)
    same_one = (joined_docs[1:-1] == doc_marks).astype(jnp.float32)[:, None]
    same_two = (joined_docs[:-2] == doc_marks).astype(jnp.float32)[:, None]
    conv_sum = (
        conv_taps[2] * joined_rows[2:]
        + conv_taps[1] * joined_rows[1:-1] * same_one
        + conv_taps[0] * joined_rows[:-2] * same_two
    )
    mixed = (outer_gate.astype(jnp.float32) * conv_sum).astype(jnp.bfloat16)
    piece_f = gather_directly(mixed, "tp", 1).astype(jnp.float32)
    scaled = (piece_f * mixer_gain).astype(jnp.bfloat16)
    accum = jnp.dot(scaled, output_weight, preferred_element_type=jnp.float32)
    squares = jnp.sum(piece_f * piece_f, axis=1)
    mix_scale = lax.rsqrt(squares / mixer_gain.shape[0] + EPS)
    hidden_state = residual_in.astype(jnp.float32) + accum * mix_scale[:, None]
    feature_total = over_copies(jnp.sum(hidden_state * hidden_state, axis=1), "tp")
    model_width = local_features * lax.axis_size("tp")
    normed = (
        hidden_state * lax.rsqrt(feature_total / model_width + EPS)[:, None] * ffn_gain
    ).astype(jnp.bfloat16)
    experts = lax.axis_size("sp") * expert_gate.shape[0]
    capacity = 4 * tokens_here // experts
    target, owners = slot_tables(routes, experts, capacity)
    padded = jnp.concatenate([normed, jnp.zeros((1, local_features), jnp.bfloat16)], axis=0)
    outgoing = padded[owners].reshape(experts, capacity, local_features)
    slices_in = lax.all_to_all(outgoing, "sp", split_axis=0, concat_axis=0, tiled=True)
    arrived = lax.all_gather(slices_in, "tp", axis=2, tiled=True)
    expert_in = arrived.reshape(-1, model_width)
    gate = jnp.dot(expert_in, expert_gate[0], preferred_element_type=jnp.float32)
    upper = jnp.dot(expert_in, expert_up[0], preferred_element_type=jnp.float32)
    act = (jax.nn.silu(gate) * upper).astype(jnp.bfloat16)
    partial_out = jnp.dot(act, expert_down[0], preferred_element_type=jnp.float32)
    summed = lax.psum_scatter(
        partial_out.astype(jnp.bfloat16), "tp", scatter_dimension=1, tiled=True
    )
    returned = lax.all_to_all(
        summed.reshape(experts, capacity, local_features),
        "sp",
        split_axis=0,
        concat_axis=0,
        tiled=True,
    )
    picked = returned.reshape(experts * capacity, local_features)[target].astype(jnp.float32)
    picked = picked.reshape(tokens_here, 2, local_features)
    routed = jnp.sum(picked * route_weights[:, :, None], axis=1)
    return (hidden_state + routed).astype(jnp.bfloat16)


def solution(mesh):
    placed = (
        P("sp", "tp"),
        P("sp", "tp"),
        P("sp", "tp"),
        P("sp", "tp"),
        P("sp"),
        P(None, "tp"),
        P(),
        P(None, "tp"),
        P("tp"),
        P("sp", None),
        P("sp", None),
        P("sp", None, "tp"),
        P("sp", None, "tp"),
        P("sp", "tp", None),
    )
    return jax.shard_map(
        per_device, mesh=mesh, in_specs=placed, out_specs=P("sp", "tp"), check_vma=False
    )
```

profile of v0, /device:TPU:1, one launch (start us, length us, event | category | flops | bytes accessed | tf_op | source)
XLA Modules:
  0.0 252.4 jit_solution(10328017283454354348)
XLA Ops:
  6.5 0.8 convert_element_type.78
  7.3 0.1 slice.41
  7.4 4.5 %collective-permute-start.1 = (bf16[2]{0:T(256)(128)(2,1)S(1)}, bf16[2]{0:T(256)(128)(2,1)S(1)}, u32[]{:S(2)}, u32[]{:S(2)}) collective-permute-start(bf16[2]{0:T(256)(128)(2,1)S(1)} %slice.41), channel_id=1, source_target_pairs={{0,4},{4,8},{8,12},{12,16},{16,20},{20,24},{24,28},{28,32},{32,36}... | collective-permute-start | bytes 20 | tf_op jit(solution)/shard_map/ppermute | solution.py:12
  11.9 0.9 multiply_convert_fusion.2
  12.8 1.9 collective-permute-start
  14.7 0.8 copy.31
  15.5 0.1 eq.37
  15.7 0.1 eq.33
  15.8 0.7 broadcast_multiply_fusion
  16.5 0.8 slice_bitcast_fusion.2
  17.3 1.2 reduce-window.6
  18.5 0.2 slice_reduce_fusion
  18.8 0.1 copy.30
  18.9 0.1 mul.153
  19.1 0.1 fusion.11
  19.2 0.1 pad_maximum_fusion
  19.3 0.8 compare_convert_fusion.1
  20.1 1.0 fusion.15
  21.1 0.1 copy.28
  21.2 0.7 broadcast_in_dim.8
  21.9 4.2 %all-to-all-start = ((bf16[4,256,128]{1,2,0:T(8,128)(2,1)}), bf16[4,256,128]{1,2,0:T(8,128)(2,1)S(1)}, u32[]{:S(2)}, u32[]{:S(2)}) async-start(bf16[4,256,128]{1,2,0:T(8,128)(2,1)} %broadcast_in_dim.8), calls=%async_computation | async-start | bytes 524288 | tf_op jit(solution)/shard_map/all_to_all | solution.py:23
  26.1 2.4 scatter_custom_fusion
  28.5 3.2 %all-to-all-done = bf16[4,256,128]{1,2,0:T(8,128)(2,1)S(1)} async-done(((bf16[4,256,128]{1,2,0:T(8,128)(2,1)}), bf16[4,256,128]{1,2,0:T(8,128)(2,1)S(1)}, u32[]{:S(2)}, u32[]{:S(2)}) %all-to-all-start) | async-done | bytes 262176 | tf_op jit(solution)/shard_map/all_to_all | solution.py:23
  31.8 0.1 multiply_reduce_fusion.2
  31.9 0.8 fusion.8
  32.7 0.4 multiply_reduce_fusion.1
  33.2 0.6 broadcast_in_dim.9
  33.8 3.2 %all-to-all-start.1 = ((f32[4,1,256]{2,1,0:T(1,128)}), f32[4,1,256]{2,1,0:T(1,128)S(1)}, u32[]{:S(2)}, u32[]{:S(2)}) async-start(f32[4,1,256]{2,1,0:T(1,128)} %broadcast_in_dim.9), calls=%async_computation.1 | async-start | bytes 8192 | tf_op jit(solution)/shard_map/all_to_all | solution.py:23
  37.0 0.0 all-gather.2.cloned.1.call-start
  37.1 4.0 %all-to-all-done.1 = f32[4,1,256]{2,1,0:T(1,128)S(1)} async-done(((f32[4,1,256]{2,1,0:T(1,128)}), f32[4,1,256]{2,1,0:T(1,128)S(1)}, u32[]{:S(2)}, u32[]{:S(2)}) %all-to-all-start.1) | async-done | bytes 4128 | tf_op jit(solution)/shard_map/all_to_all | solution.py:23
  41.2 0.1 multiply_convert_fusion.1
  41.3 4.0 %gather_fusion = bf16[1024,512]{1,0:T(8,128)(2,1)S(1)} fusion(bf16[257,512]{1,0:T(8,128)(2,1)S(1)} %concatenate.11, s32[1024]{0:T(1024)S(1)} %fusion.19), kind=kCustom, calls=%fused_computation | custom fusion | bytes 2101248 | tf_op jit(solution)/shard_map/gather | solution.py:97
  45.3 42.3 %all_to_all.21 = bf16[64,16,512]{2,1,0:T(8,128)(2,1)} all-to-all(bf16[64,16,512]{2,1,0:T(8,128)(2,1)S(1)} %bitcast.54), channel_id=1, replica_groups=mesh['sp'=64,'tp'=4] {'sp'}, dimensions={0} | all-to-all | bytes 2097152 | tf_op jit(solution)/shard_map/all_to_all | solution.py:98
  87.6 0.0 all-gather.2.cloned.1.call-update
  87.7 0.0 reduce-scatter.2.cloned.1.call-start
  87.7 45.8 %all-gather.2.cloned.1.call-done = bf16[64,16,2048]{2,1,0:T(8,128)(2,1)} async-done(((bf16[64,16,512]{2,1,0:T(8,128)(2,1)}), bf16[64,16,2048]{2,1,0:T(8,128)(2,1)}) %all-gather.2.cloned.1.call-update) | async-done | bytes 4194320 | tf_op jit(solution)/shard_map/all_gather | solution.py:99
  133.5 7.5 %fusion.1 = f32[1024,896]{1,0:T(8,128)S(1)} fusion(bf16[1024,2048]{1,0:T(8,128)(2,1)} %bitcast.59, bf16[1,2048,896]{2,1,0:T(8,128)(2,1)} %param.26), kind=kOutput, calls=%fused_computation.5 | convolution fusion | flops 3758096384 | bytes 11534336 | tf_op jit(solution)/shard_map/dot_general | solution.py:102
  141.0 4.8 %multiply_convert_fusion = bf16[1024,896]{1,0:T(8,128)(2,1)S(1)} fusion(f32[1024,896]{1,0:T(8,128)S(1)} %fusion.1, bf16[1024,2048]{1,0:T(8,128)(2,1)S(1)} %bitcast.60, bf16[1,2048,896]{2,1,0:T(8,128)(2,1)S(1)} %copy-done.5), kind=kOutput, calls=%fused_computation.9 | convolution fusion | flops 3763601408 | bytes 13369344 | tf_op jit(solution)/shard_map/dot_general | solution.py:101
  145.9 6.1 %convolution_convert_fusion = bf16[1024,2048]{1,0:T(8,128)(2,1)} fusion(bf16[1024,896]{1,0:T(8,128)(2,1)S(1)} %multiply_convert_fusion, bf16[1,896,2048]{2,1,0:T(8,128)(2,1)S(1)} %copy-done.6), kind=kOutput, calls=%fused_computation.3 | convolution fusion | flops 3760193536 | bytes 9699328 | tf_op jit(solution)/shard_map/dot_general | solution.py:104
  151.9 0.0 reduce-scatter.2.cloned.1.call-update
  151.9 50.0 %reduce-scatter.2.cloned.1.call-done = bf16[1024,512]{1,0:T(8,128)(2,1)} async-done(((bf16[1024,2048]{1,0:T(8,128)(2,1)}), bf16[1024,512]{1,0:T(8,128)(2,1)}) %reduce-scatter.2.cloned.1.call-update) | async-done | bytes 1048592 | tf_op jit(solution)/shard_map/reduce_scatter | solution.py:105
  202.0 10.7 %all-to-all-start.3 = ((bf16[64,16,512]{2,1,0:T(8,128)(2,1)}), bf16[64,16,512]{2,1,0:T(8,128)(2,1)S(1)}, u32[]{:S(2)}, u32[]{:S(2)}) async-start(bf16[64,16,512]{2,1,0:T(8,128)(2,1)} %bitcast.55), calls=%async_computation.4 | async-start | bytes 2097152 | tf_op jit(solution)/shard_map/all_to_all | solution.py:108
  212.7 0.1 copy.34
  212.8 28.0 %all-to-all-done.3 = bf16[64,16,512]{2,1,0:T(8,128)(2,1)S(1)} async-done(((bf16[64,16,512]{2,1,0:T(8,128)(2,1)}), bf16[64,16,512]{2,1,0:T(8,128)(2,1)S(1)}, u32[]{:S(2)}, u32[]{:S(2)}) %all-to-all-start.3) | async-done | bytes 1048608 | tf_op jit(solution)/shard_map/all_to_all | solution.py:108
  240.8 2.0 gather_fusion.1
  242.8 0.7 reshape.90
  243.5 1.3 multiply_reduce_fusion
  244.8 0.8 add_convert_fusion
  (29 shorter events, 0.2 us)
Async XLA Ops:
  6.5 26.2 %copy-start = (bf16[512,512]{1,0:T(8,128)(2,1)S(1)}, bf16[512,512]{1,0:T(8,128)(2,1)}, u32[]{:S(2)}) copy-start(bf16[512,512]{1,0:T(8,128)(2,1)} %param.21) | copy-start | bytes 1572868
  6.5 26.2 %copy-start.1 = (bf16[256,512]{1,0:T(8,128)(2,1)S(1)}, bf16[256,512]{1,0:T(8,128)(2,1)}, u32[]{:S(2)}) copy-start(bf16[256,512]{1,0:T(8,128)(2,1)} %param.14) | copy-start | bytes 786436
  6.5 34.6 %copy-start.2 = (f32[512]{0:T(512)S(1)}, f32[512]{0:T(512)}, u32[]{:S(2)}) copy-start(f32[512]{0:T(512)} %param.22) | copy-start | bytes 6148
  7.4 11.8 %collective-permute-start.1 = (bf16[2]{0:T(256)(128)(2,1)S(1)}, bf16[2]{0:T(256)(128)(2,1)S(1)}, u32[]{:S(2)}, u32[]{:S(2)}) collective-permute-start(bf16[2]{0:T(256)(128)(2,1)S(1)} %slice.41), channel_id=1, source_target_pairs={{0,4},{4,8},{8,12},{12,16},{16,20},{20,24},{24,28},{28,32},{32,36}... | collective-permute-start | bytes 20 | tf_op jit(solution)/shard_map/ppermute | solution.py:12
  12.8 7.3 %collective-permute-start = (bf16[2,128]{1,0:T(2,128)(2,1)S(1)}, bf16[2,128]{1,0:T(2,128)(2,1)S(1)}, u32[]{:S(2)}, u32[]{:S(2)}) collective-permute-start(bf16[2,128]{1,0:T(2,128)(2,1)S(1)} %slice.52), channel_id=1, source_target_pairs={{0,4},{4,8},{8,12},{12,16},{16,20},{20,24},{24,28},{28,32},{32,36}... | collective-permute-start | bytes 1544 | tf_op jit(solution)/shard_map/ppermute | solution.py:12
  21.9 9.9 %all-to-all-start = ((bf16[4,256,128]{1,2,0:T(8,128)(2,1)}), bf16[4,256,128]{1,2,0:T(8,128)(2,1)S(1)}, u32[]{:S(2)}, u32[]{:S(2)}) async-start(bf16[4,256,128]{1,2,0:T(8,128)(2,1)} %broadcast_in_dim.8), calls=%async_computation | async-start | bytes 524288 | tf_op jit(solution)/shard_map/all_to_all | solution.py:23
  33.8 7.4 %all-to-all-start.1 = ((f32[4,1,256]{2,1,0:T(1,128)}), f32[4,1,256]{2,1,0:T(1,128)S(1)}, u32[]{:S(2)}, u32[]{:S(2)}) async-start(f32[4,1,256]{2,1,0:T(1,128)} %broadcast_in_dim.9), calls=%async_computation.1 | async-start | bytes 8192 | tf_op jit(solution)/shard_map/all_to_all | solution.py:23
  37.0 96.5 %all-gather.2.cloned.1.call-start = ((), (), s32[]{:S(2)}) async-start(), calls=%async_computation.5 | async-start | bytes 5242880 | tf_op jit(solution)/shard_map/all_gather | solution.py:99
  87.7 114.3 %reduce-scatter.2.cloned.1.call-start = ((), (), s32[]{:S(2)}) async-start(), calls=%async_computation.6 | async-start | bytes 5242880 | tf_op jit(solution)/shard_map/reduce_scatter | solution.py:105
  133.5 7.5 %copy-start.4 = (bf16[64,16,2048]{2,1,0:T(8,128)(2,1)S(1)}, bf16[64,16,2048]{2,1,0:T(8,128)(2,1)}, u32[]{:S(2)}) copy-start(bf16[64,16,2048]{2,1,0:T(8,128)(2,1)} %all-gather.2.cloned.1.call-done) | copy-start | bytes 12582916
  133.5 7.5 %copy-start.5 = (bf16[1,2048,896]{2,1,0:T(8,128)(2,1)S(1)}, bf16[1,2048,896]{2,1,0:T(8,128)(2,1)}, u32[]{:S(2)}) copy-start(bf16[1,2048,896]{2,1,0:T(8,128)(2,1)} %param.25) | copy-start | bytes 11010052
  141.0 4.8 %copy-start.6 = (bf16[1,896,2048]{2,1,0:T(8,128)(2,1)S(1)}, bf16[1,896,2048]{2,1,0:T(8,128)(2,1)}, u32[]{:S(2)}) copy-start(bf16[1,896,2048]{2,1,0:T(8,128)(2,1)} %param.27) | copy-start | bytes 11010052
  151.9 60.8 %copy-start.3 = (f32[256,2]{0,1:T(2,128)S(1)}, f32[256,2]{0,1:T(2,128)}, u32[]{:S(2)}) copy-start(f32[256,2]{0,1:T(2,128)} %param.24) | copy-start | bytes 6148
  202.0 38.9 %all-to-all-start.3 = ((bf16[64,16,512]{2,1,0:T(8,128)(2,1)}), bf16[64,16,512]{2,1,0:T(8,128)(2,1)S(1)}, u32[]{:S(2)}, u32[]{:S(2)}) async-start(bf16[64,16,512]{2,1,0:T(8,128)(2,1)} %bitcast.55), calls=%async_computation.4 | async-start | bytes 2097152 | tf_op jit(solution)/shard_map/all_to_all | solution.py:108
Sparse Core Ops, SparseCore 0:
  87.8 45.6 all-gather.1
  152.1 49.8 reduce-scatter.1
where the time goes:
time: 253 us; the launch traced here: 252 us
  waiting for transfers between devices  131 us (52%)
  blocking collectives  42.3 us (17%)
  starting transfers between devices  24.6 us (10%)
  matrix products  18.8 us (7%)
  between operations  13.7 us (5%)
  local copies, waits for them, and re-layouts  13.1 us (5%)
  other arithmetic  8.73 us (3%)
    reduce_scatter x1, waiting for transfers between devices, per_device(): lax.psum_scatter(partial_out.astype(jnp.bfloat16), 'tp', scatter_dimensio...  50 us
    all_gather x1, waiting for transfers between devices, per_device(): arrived = lax.all_gather(slices_in, 'tp', axis=2, tiled=True)  45.8 us
    all_to_all x1, blocking collectives, per_device(): lax.all_to_all(outgoing, 'sp', split_axis=0, concat_axis=0, tiled=True)  42.3 us
    all_to_all x1, waiting for transfers between devices, per_device(): lax.all_to_all(summed.reshape(experts, capacity, local_features), 'sp', s...  28 us
    all_to_all x1, starting transfers between devices, per_device(): lax.all_to_all(summed.reshape(experts, capacity, local_features), 'sp', s...  10.7 us
    dot_general x1, matrix products, per_device(): upper = jnp.dot(expert_in, expert_up[0], preferred_element_type=jnp.float32)  7.49 us
    all_to_all x2, starting transfers between devices, sent_to_all(): return lax.all_to_all(copies, axis, split_axis=0, concat_axis=0, tiled=True)  7.43 us
    all_to_all x2, waiting for transfers between devices, sent_to_all(): return lax.all_to_all(copies, axis, split_axis=0, concat_axis=0, tiled=True)  7.29 us
  transfers between devices with their start and end apart: 7, of which 5 were waited for; matrix products, arithmetic and copies ran while one was open for 3% of the time, Pallas kernels for 0%

commit v1 on v0

v1 whole, which is shorter than its diff:
```python
import functools

import jax
import jax.numpy as jnp
from jax import lax
from jax.experimental import pallas as pl
from jax.experimental.pallas import tpu as pltpu
from jax.sharding import PartitionSpec as P

EPS = 1e-06
CORES = 2
NX = 4
MESH = pl.DeviceIdType.MESH
F32 = jnp.float32
BF16 = jnp.bfloat16


def layer_kernel(
    nsp,
    ntp,
    cap,
    res_h,
    ci_h,
    og_h,
    ig_h,
    doc_h,
    taps_h,
    mg_h,
    ow_h,
    fg_h,
    rt_h,
    rw_h,
    wg_h,
    wu_h,
    wd_h,
    out_ref,
    res,
    ci,
    og,
    ig,
    doc,
    taps,
    mg,
    ow,
    fg,
    rt,
    rw,
    wg,
    wu,
    wd,
    rows8,
    cols8,
    joined,
    docj,
    halo_out,
    halo_in,
    mix,
    ss,
    hid,
    perm,
    outgo,
    xin,
    act,
    part,
    ra,
    rb,
    fl,
    fr,
    ret,
    ret_in,
    load_sem,
    halo_sem,
    mix_s,
    mix_r,
    ss_s,
    ss_r,
    disp_s,
    disp_r,
    ag_s,
    ag_r,
    rs_s,
    rs_r,
    ret_s,
    ret_r,
):
    sp = lax.axis_index("sp")
    tp = lax.axis_index("tp")
    nz = nsp // (NX * CORES)
    zpos = sp // (NX * CORES)
    xpos = (sp // CORES) % NX
    cpos = sp % CORES
    tokens, features = res.shape
    channels = ci.shape[1]
    group = nz * CORES * cap
    half = group // 2
    pair = CORES * cap
    left = lax.rem(tp + ntp - 1, ntp)
    right = lax.rem(tp + 1, ntp)
    opposite = lax.rem(tp + 2, ntp)

    barrier = pltpu.get_barrier_semaphore()

    def greet(step, carry):
        pl.semaphore_signal(
            barrier,
            inc=1,
            device_id=(lax.rem(sp + step, nsp), tp),
            device_id_type=MESH,
        )
        return carry

    lax.fori_loop(1, nsp, greet, 0)
    for d in range(1, ntp):
        pl.semaphore_signal(
            barrier, inc=1, device_id=(sp, lax.rem(tp + d, ntp)), device_id_type=MESH
        )

    pairs = (
        (rt_h, rt),
        (doc_h, doc),
        (rw_h, rw),
        (ci_h, ci),
        (ig_h, ig),
        (og_h, og),
        (taps_h, taps),
        (mg_h, mg),
        (ow_h, ow),
        (res_h, res),
        (fg_h, fg),
        (wg_h.at[0], wg),
        (wu_h.at[0], wu),
        (wd_h.at[0], wd),
    )
    loads = [
        pltpu.make_async_copy(src, dst, load_sem.at[i]) for i, (src, dst) in enumerate(pairs)
    ]
    for load in loads:
        load.start()

    for i in range(3):
        loads[i].wait()
    experts_iota = lax.broadcasted_iota(jnp.int32, (nsp, tokens), 0)
    first = (experts_iota == rt[0:1, :]).astype(F32)
    second = (experts_iota == rt[1:2, :]).astype(F32)
    named = (first + second).astype(BF16)
    before = (
        lax.broadcasted_iota(jnp.int32, (tokens, tokens), 0)
        < lax.broadcasted_iota(jnp.int32, (tokens, tokens), 1)
    ).astype(F32).astype(BF16)
    earlier = jnp.dot(named, before, preferred_element_type=F32)
    slots = earlier + (experts_iota * cap).astype(F32)
    rows8[0:1, :] = doc[...].astype(F32)
    rows8[1:2, :] = jnp.sum(first * slots, axis=0, keepdims=True)
    rows8[2:3, :] = jnp.sum(second * slots, axis=0, keepdims=True)
    rows8[3:5, :] = rw[...]
    rows8[5:8, :] = jnp.zeros((3, tokens), F32)
    cols8[...] = jnp.transpose(rows8[...])

    loads[3].wait()
    loads[4].wait()
    value = (ig[...].astype(F32) * ci[...].astype(F32)).astype(BF16).astype(F32)
    joined[8:, :] = value
    docj[8:, :] = jnp.broadcast_to(cols8[:, 0:1], (tokens, channels))
    halo_out[0:8, :] = value[tokens - 8 :, :]
    halo_out[8:16, :] = jnp.broadcast_to(cols8[tokens - 8 :, 0:1], (8, channels))

    pl.semaphore_wait(barrier, nsp + ntp - 2)
    halo = pltpu.make_async_remote_copy(
        src_ref=halo_out,
        dst_ref=halo_in,
        send_sem=halo_sem.at[0],
        recv_sem=halo_sem.at[1],
        device_id=(lax.rem(sp + 1, nsp), tp),
        device_id_type=MESH,
    )
    halo.start()

    line = lax.broadcasted_iota(jnp.int32, (group, tokens), 0)
    spread = (line // pair) * (NX * pair) + lax.rem(line, pair)
    for j in range(NX):
        slot = (spread + lax.rem(xpos + j, NX) * pair).astype(F32)
        hit = (slot == rows8[1:2, :]) | (slot == rows8[2:3, :])
        perm[j] = hit.astype(F32).astype(BF16)

    for i in range(5, 7):
        loads[i].wait()
    halo.wait()
    joined[0:8, :] = halo_in[0:8, :]
    docj[0:8, :] = jnp.where(sp == 0, -1.0, halo_in[8:16, :])
    docs_now = docj[8:, :]
    same_one = (docj[7 : tokens + 7, :] == docs_now).astype(F32)
    same_two = (docj[6 : tokens + 6, :] == docs_now).astype(F32)
    conv_sum = (
        taps[2:3, :] * joined[8:, :]
        + taps[1:2, :] * joined[7 : tokens + 7, :] * same_one
        + taps[0:1, :] * joined[6 : tokens + 6, :] * same_two
    )
    mix[tp] = (og[...].astype(F32) * conv_sum).astype(BF16)

    def to_tp(buffer, send, recv):
        copies = []
        for d in (1, ntp - 1, *range(2, ntp - 1)):
            copies.append(
                pltpu.make_async_remote_copy(
                    src_ref=buffer.at[tp],
                    dst_ref=buffer.at[tp],
                    send_sem=send.at[d - 1],
                    recv_sem=recv.at[d - 1],
                    device_id=(sp, lax.rem(tp + d, ntp)),
                    device_id_type=MESH,
                )
            )
        for copy in copies:
            copy.start()
        return copies

    mix_copies = to_tp(mix, mix_s, mix_r)
    for i in range(7, 11):
        loads[i].wait()
    for copy in mix_copies:
        copy.wait()
    pieces = jnp.concatenate([mix[q] for q in range(ntp)], axis=1).astype(F32)
    squares = jnp.sum(pieces * pieces, axis=1, keepdims=True)
    mix_scale = lax.rsqrt(squares / (channels * ntp) + EPS)
    scaled = (pieces * mg[...]).astype(BF16)
    projected = jnp.dot(scaled, ow[...], preferred_element_type=F32)
    hidden = res[...].astype(F32) + projected * mix_scale
    hid[...] = hidden
    power = hidden * hidden
    folded = power[:, 0:128]
    for k in range(1, features // 128):
        folded = folded + power[:, k * 128 : (k + 1) * 128]
    ss[tp] = jnp.broadcast_to(
        jnp.sum(jnp.transpose(folded), axis=0, keepdims=True), (8, tokens)
    )
    ss_copies = to_tp(ss, ss_s, ss_r)
    for copy in ss_copies:
        copy.wait()
    total = ss[0]
    for q in range(1, ntp):
        total = total + ss[q]
    scale = jnp.transpose(lax.rsqrt(total / (features * ntp) + EPS))[:, 0:1]
    normed = (hid[...] * scale * fg[...]).astype(BF16)

    mine = pl.multiple_of((zpos * CORES + cpos) * cap, cap)

    def exchange(src, dst, send, recv, j, xx):
        def one(zz, cc):
            at = pl.multiple_of((zz * CORES + cc) * cap, cap)
            pltpu.make_async_remote_copy(
                src_ref=src.at[j, pl.ds(at, cap)],
                dst_ref=dst(j, mine),
                send_sem=send.at[j],
                recv_sem=recv.at[j],
                device_id=((zz * NX + xx) * CORES + cc, tp),
                device_id_type=MESH,
            ).start()

        def far(i, carry):
            h = i // 2 + 1
            k = jnp.where(lax.rem(i, 2) == 0, h, nz - h)
            zz = lax.rem(zpos + k, nz)
            for cc in range(CORES):
                one(zz, cc)
            return carry

        lax.fori_loop(0, nz - 1, far, 0)
        if j == 0:
            one(zpos, 1 - cpos)
        else:
            for cc in range(CORES):
                one(zpos, cc)

    def rows_of(j):
        return group - cap if j == 0 else group

    for j in range(NX):
        outgo[j] = jnp.dot(perm[j], normed, preferred_element_type=F32).astype(BF16)
        if j == 0:
            xin[tp, 0, pl.ds(mine, cap), :] = outgo[0, pl.ds(mine, cap), :]
        exchange(
            outgo,
            lambda j, at: xin.at[tp, j, pl.ds(at, cap)],
            disp_s,
            disp_r,
            j,
            lax.rem(xpos + j, NX),
        )

    def tp_copy(src, dst, send, recv, to):
        return pltpu.make_async_remote_copy(
            src_ref=src,
            dst_ref=dst,
            send_sem=send,
            recv_sem=recv,
            device_id=(sp, to),
            device_id_type=MESH,
        )

    upper = pl.ds(0, half)
    lower = pl.ds(half, half)

    def got(ref, sem):
        pltpu.make_async_copy(ref, ref, sem).wait()

    def own(j):
        got(xin.at[tp, j, pl.ds(0, rows_of(j))], disp_r.at[j])
        tp_copy(xin.at[tp, j], xin.at[tp, j], ag_s.at[0, j], ag_r.at[0, j], right).start()
        tp_copy(xin.at[tp, j], xin.at[tp, j], ag_s.at[1, j], ag_r.at[1, j], left).start()

    def forward(j):
        got(xin.at[left, j], ag_r.at[0, j])
        ref = xin.at[left, j, upper]
        tp_copy(ref, ref, ag_s.at[2, j], ag_r.at[2, j], right).start()
        got(xin.at[right, j], ag_r.at[1, j])
        ref = xin.at[right, j, lower]
        tp_copy(ref, ref, ag_s.at[3, j], ag_r.at[3, j], left).start()

    hidden_units = wg.shape[1]
    tile = 128
    wide = 256
    per_q = features // wide

    def experts(j):
        got(xin.at[opposite, j, upper], ag_r.at[2, j])
        got(xin.at[opposite, j, lower], ag_r.at[3, j])

        def up_tile(n, carry):
            at = pl.ds(pl.multiple_of(n * tile, tile), tile)
            rows = jnp.concatenate([xin[q, j] for q in range(ntp)], axis=1)
            both = jnp.concatenate([wg[:, at], wu[:, at]], axis=1)
            made = jnp.dot(rows, both, preferred_element_type=F32)
            gate = made[:, :tile]
            act[:, at] = (jax.nn.silu(gate) * made[:, tile:]).astype(BF16)
            return carry

        lax.fori_loop(0, hidden_units // tile, up_tile, 0)
        for q in range(ntp):
            for k in range(per_q):
                cols = slice(q * features + k * wide, q * features + (k + 1) * wide)
                part[j, q, :, k * wide : (k + 1) * wide] = jnp.dot(
                    act[...], wd[:, cols], preferred_element_type=F32
                ).astype(BF16)
        tp_copy(part.at[j, opposite, upper], ra.at[j], rs_s.at[0, j], rs_r.at[0, j], right).start()
        tp_copy(part.at[j, opposite, lower], rb.at[j], rs_s.at[1, j], rs_r.at[1, j], left).start()
        tp_copy(
            part.at[j, right, lower], fl.at[j, lower], rs_s.at[2, j], rs_r.at[2, j], right
        ).start()
        tp_copy(
            part.at[j, left, upper], fr.at[j, upper], rs_s.at[3, j], rs_r.at[3, j], left
        ).start()

    def add_on(j):
        got(ra.at[j], rs_r.at[0, j])
        part[j, right, upper, :] = (
            part[j, right, upper, :].astype(F32) + ra[j].astype(F32)
        ).astype(BF16)
        tp_copy(
            part.at[j, right, upper], fl.at[j, upper], rs_s.at[4, j], rs_r.at[4, j], right
        ).start()
        got(rb.at[j], rs_r.at[1, j])
        part[j, left, lower, :] = (
            part[j, left, lower, :].astype(F32) + rb[j].astype(F32)
        ).astype(BF16)
        tp_copy(
            part.at[j, left, lower], fr.at[j, lower], rs_s.at[5, j], rs_r.at[5, j], left
        ).start()

    def give_back(j):
        got(fl.at[j, lower], rs_r.at[2, j])
        got(fr.at[j, upper], rs_r.at[3, j])
        got(fl.at[j, upper], rs_r.at[4, j])
        got(fr.at[j, lower], rs_r.at[5, j])
        ret[j] = (part[j, tp].astype(F32) + fl[j].astype(F32) + fr[j].astype(F32)).astype(BF16)
        if j == 0:
            ret_in[0, pl.ds(mine, cap), :] = ret[0, pl.ds(mine, cap), :]
        exchange(
            ret,
            lambda j, at: ret_in.at[j, pl.ds(at, cap)],
            ret_s,
            ret_r,
            j,
            lax.rem(xpos + NX - j, NX),
        )

    own(0)
    own(1)
    forward(0)
    own(2)
    forward(1)
    for i in range(11, 14):
        loads[i].wait()
    experts(0)
    own(3)
    forward(2)
    add_on(0)
    experts(1)
    forward(3)
    give_back(0)
    add_on(1)
    experts(2)
    give_back(1)
    add_on(2)
    experts(3)
    give_back(2)
    add_on(3)
    give_back(3)

    lane = lax.broadcasted_iota(jnp.int32, (tokens, group), 1)
    spread = (lane // pair) * (NX * pair) + lax.rem(lane, pair)
    for j in range(NX):
        got(ret_in.at[j, pl.ds(0, rows_of(j))], ret_r.at[j])
        slot = (spread + lax.rem(xpos + j, NX) * pair).astype(F32)
        routed = hid[...]
        for k in range(2):
            pick = (slot == cols8[:, 1 + k : 2 + k]).astype(F32).astype(BF16)
            routed = routed + cols8[:, 3 + k : 4 + k] * jnp.dot(
                pick, ret_in[j], preferred_element_type=F32
            )
        hid[...] = routed
    out_ref[...] = hid[...].astype(BF16)

    for j in range(NX):
        got(outgo.at[j, pl.ds(0, rows_of(j))], disp_s.at[j])
        got(ret.at[j, pl.ds(0, rows_of(j))], ret_s.at[j])
        for i in range(2):
            got(xin.at[tp, j], ag_s.at[i, j])
        for i in range(2, 4):
            got(xin.at[tp, j, upper], ag_s.at[i, j])
        for i in range(6):
            got(part.at[j, 0, upper], rs_s.at[i, j])


def per_device(
    residual_in,
    conv_input,
    outer_gate,
    inner_gate,
    documents,
    conv_taps,
    mixer_gain,
    output_weight,
    ffn_gain,
    routes,
    route_weights,
    expert_gate,
    expert_up,
    expert_down,
):
    nsp = lax.axis_size("sp")
    ntp = lax.axis_size("tp")
    tokens, features = residual_in.shape
    channels = conv_input.shape[1]
    cap = 4 * tokens // nsp
    group = nsp // NX * cap
    half = group // 2
    width = features * ntp
    hidden_units = expert_gate.shape[2]
    args = (
        residual_in,
        conv_input,
        outer_gate,
        inner_gate,
        documents.reshape(1, tokens),
        conv_taps,
        mixer_gain.reshape(1, -1),
        output_weight,
        ffn_gain.reshape(1, -1),
        routes.T,
        route_weights.T,
        expert_gate,
        expert_up,
        expert_down,
    )
    locals_ = [
        pltpu.VMEM(a.shape if a.ndim == 2 else a.shape[1:], a.dtype) for a in args
    ]
    dma = pltpu.SemaphoreType.DMA
    scratch = locals_ + [
        pltpu.VMEM((8, tokens), F32),
        pltpu.VMEM((tokens, 8), F32),
        pltpu.VMEM((tokens + 8, channels), F32),
        pltpu.VMEM((tokens + 8, channels), F32),
        pltpu.VMEM((16, channels), F32),
        pltpu.VMEM((16, channels), F32),
        pltpu.VMEM((ntp, tokens, channels), BF16),
        pltpu.VMEM((ntp, 8, tokens), F32),
        pltpu.VMEM((tokens, features), F32),
        pltpu.VMEM((NX, group, tokens), BF16),
        pltpu.VMEM((NX, group, features), BF16),
        pltpu.VMEM((ntp, NX, group, features), BF16),
        pltpu.VMEM((group, hidden_units), BF16),
        pltpu.VMEM((NX, ntp, group, features), BF16),
        pltpu.VMEM((NX, half, features), BF16),
        pltpu.VMEM((NX, half, features), BF16),
        pltpu.VMEM((NX, group, features), BF16),
        pltpu.VMEM((NX, group, features), BF16),
        pltpu.VMEM((NX, group, features), BF16),
        pltpu.VMEM((NX, group, features), BF16),
        dma((len(args),)),
        dma((2,)),
        dma((ntp - 1,)),
        dma((ntp - 1,)),
        dma((ntp - 1,)),
        dma((ntp - 1,)),
        dma((NX,)),
        dma((NX,)),
        dma((4, NX)),
        dma((4, NX)),
        dma((6, NX)),
        dma((6, NX)),
        dma((NX,)),
        dma((NX,)),
    ]
    return pl.pallas_call(
        functools.partial(layer_kernel, nsp, ntp, cap),
        out_shape=jax.ShapeDtypeStruct((tokens, features), BF16),
        in_specs=[pl.BlockSpec(memory_space=pl.ANY)] * len(args),
        out_specs=pl.BlockSpec(memory_space=pltpu.VMEM),
        scratch_shapes=scratch,
        compiler_params=pltpu.CompilerParams(
            collective_id=0, has_side_effects=True, vmem_limit_bytes=60 * 1024 * 1024
        ),
        cost_estimate=pl.CostEstimate(
            flops=6 * nsp * cap * width * hidden_units,
            bytes_accessed=6 * width * hidden_units,
            transcendentals=0,
        ),
        name="layer",
    )(*args)


def solution(mesh):
    placed = (
        P("sp", "tp"),
        P("sp", "tp"),
        P("sp", "tp"),
        P("sp", "tp"),
        P("sp"),
        P(None, "tp"),
        P(),
        P(None, "tp"),
        P("tp"),
        P("sp", None),
        P("sp", None),
        P("sp", None, "tp"),
        P("sp", None, "tp"),
        P("sp", "tp", None),
    )
    return jax.shard_map(
        per_device, mesh=mesh, in_specs=placed, out_specs=P("sp", "tp"), check_vma=False
    )
```

time: 253 us -> 117 us (0.46)
  waiting for transfers between devices: 131 us -> 0 us
  Pallas kernels: 0 us -> 115 us
  blocking collectives: 42.3 us -> 0 us
  starting transfers between devices: 24.6 us -> 0 us
  matrix products: 18.8 us -> 0 us
  between operations: 13.7 us -> 0.01 us
  local copies, waits for them, and re-layouts: 13.1 us -> 1.67 us
  other arithmetic: 8.73 us -> 0 us
    pallas_call x0 -> x1, Pallas kernels: none -> 115 us  [per_device(): pl.pallas_call(functools.partial(layer_kernel, nsp, ntp, cap), out_shape=...]
    reduce_scatter x1 -> x0, waiting for transfers between devices: 50 us -> none  [per_device(): lax.psum_scatter(partial_out.astype(jnp.bfloat16), 'tp', scatter_dimensio...]
    all_gather x1 -> x0, waiting for transfers between devices: 45.8 us -> none  [per_device(): arrived = lax.all_gather(slices_in, 'tp', axis=2, tiled=True)]
    all_to_all x1 -> x0, blocking collectives: 42.3 us -> none  [per_device(): lax.all_to_all(outgoing, 'sp', split_axis=0, concat_axis=0, tiled=True)]
    all_to_all x3 -> x0, waiting for transfers between devices: 35.3 us -> none  [the longest x1 28 us: per_device(): lax.all_to_all(summed.reshape(experts, capacity, local_features), 'sp', s...]
    dot_general x4 -> x0, matrix products: 18.8 us -> none  [the longest x1 7.49 us: per_device(): upper = jnp.dot(expert_in, expert_up[0], preferred_element_type=jnp.float32)]
    all_to_all x3 -> x0, starting transfers between devices: 18.1 us -> none  [the longest x1 10.7 us: per_device(): lax.all_to_all(summed.reshape(experts, capacity, local_features), 'sp', s...]
    ppermute x2 -> x0, starting transfers between devices: 6.41 us -> none  [from_behind(): return lax.ppermute(block, axis, route)]
  transfers between devices with their start and end apart: 7 -> 0, of which waited for: 5 -> 0; matrix products, arithmetic and copies ran while one was open for 3% -> 0% of each run, Pallas kernels for 0% -> 0%
where the time goes in v1:
time: 117 us; the launch traced here: 116 us
  Pallas kernels  115 us (98%)
  local copies, waits for them, and re-layouts  1.67 us (1%)
    pallas_call x1, Pallas kernels, per_device(): pl.pallas_call(functools.partial(layer_kernel, nsp, ntp, cap), out_shape=...  115 us

profile of v1, /device:TPU:1, one launch (start us, length us, event | category | flops | bytes accessed | tf_op | source)
XLA Modules:
  0.0 116.4 jit_solution(4253761013291560231)
XLA Ops:
  0.0 114.7 %layer.1 = bf16[256,512]{1,0:T(8,128)(2,1)} custom-call(bf16[256,512]{1,0:T(8,128)(2,1)} %res_h.1, bf16[256,128]{1,0:T(8,128)(2,1)} %ci_h.1, bf16[256,128]{1,0:T(8,128)(2,1)} %og_h.1, bf16[256,128]{1,0:T(8,128)(2,1)} %ig_h.1, s32[1,256]{1,0:T(1,128)} %bitcast.9, f32[3,128]{1,0:T(4,128)} %taps_h.1, f32[1,512]{1,0:T(1,128)} %bitcast.5, bf16[512,512]{1,0:T(8,128)(2,1)} %ow_h.1, ...), custom_call_target="tpu_custom_call" | custom-call | flops 11274289152 | bytes 11010048 | tf_op jit(solution)/shard_map/layer/pallas_call | solution.py:515
  114.7 1.7 %copy.16 = bf16[256,512]{1,0:T(8,128)(2,1)} copy(bf16[256,512]{1,0:T(8,128)(2,1)} %layer.1) | data formatting | bytes 524288

commit v2 on v1

v2 whole, which is shorter than its diff:
```python
import functools

import jax
import jax.numpy as jnp
from jax import lax
from jax.experimental import pallas as pl
from jax.experimental.pallas import tpu as pltpu
from jax.sharding import PartitionSpec as P

EPS = 1e-06
CORES = 2
NX = 4
OFFSETS = (0, 1, -1, 2, -2, 3, -3, 4)
NEAR = 3
PIECES = ((3, 2), (5, 2), (7, 1), (1, 2), (0, 1))
ORDER = (
    ("tokens", 0),
    ("own", 0),
    ("near", 0),
    ("forward", 0),
    ("weights", 0),
    ("own", 1),
    ("up", 0),
    ("forward", 1),
    ("down", 0),
    ("own", 2),
    ("start", 0),
    ("upz", 0),
    ("downz", 0),
    ("up", 1),
    ("forward", 2),
    ("down", 1),
    ("add", 0),
    ("start", 1),
    ("up", 2),
    ("down", 2),
    ("start", 2),
    ("back", 0),
    ("upn", 0),
    ("add", 1),
    ("downn", 0),
    ("add", 2),
    ("start", 3),
    ("start", 4),
    ("back", 1),
    ("back", 2),
    ("add", 3),
    ("add", 4),
    ("combine", 0),
    ("back", 3),
    ("back", 4),
    ("combine", 1),
    ("combine", 2),
    ("gone", 0),
    ("combine", 4),
    ("combine", 3),
)
MESH = pl.DeviceIdType.MESH
F32 = jnp.float32
BF16 = jnp.bfloat16


def layer_kernel(
    nsp,
    ntp,
    cap,
    res_h,
    ci_h,
    og_h,
    ig_h,
    doc_h,
    taps_h,
    mg_h,
    ow_h,
    fg_h,
    rt_h,
    rw_h,
    wg_h,
    wu_h,
    wd_h,
    out_ref,
    res,
    ci,
    og,
    ig,
    doc,
    taps,
    mg,
    ow,
    fg,
    rt,
    rw,
    wg,
    wu,
    wd,
    rows8,
    cols8,
    joined,
    docj,
    halo_out,
    halo_in,
    gains,
    mix,
    tok,
    hid,
    perm,
    outgo,
    outrow,
    xin,
    scl,
    act,
    part,
    rx,
    fl,
    fr,
    ret,
    ret_in,
    load_sem,
    halo_sem,
    gain_s,
    gain_r,
    mix_s,
    mix_r,
    disp_s,
    disp_r,
    ag_s,
    ag_r,
    rs_s,
    rs_r,
    ret_s,
    ret_r,
    round_sem,
):
    sp = lax.axis_index("sp")
    tp = lax.axis_index("tp")
    nz = nsp // (NX * CORES)
    zpos = sp // (NX * CORES)
    xpos = (sp // CORES) % NX
    cpos = sp % CORES
    tokens, features = res.shape
    channels = ci.shape[1]
    peers = NX * CORES
    region = peers * cap
    left = lax.rem(tp + ntp - 1, ntp)
    right = lax.rem(tp + 1, ntp)
    opposite = lax.rem(tp + 2, ntp)

    def at_sp(dz, dx, core):
        return (
            lax.rem(zpos + (dz + nz), nz) * NX + lax.rem(xpos + dx, NX)
        ) * CORES + core

    def signal(sem, to):
        pl.semaphore_signal(sem, inc=1, device_id=to, device_id_type=MESH)

    barrier = pltpu.get_barrier_semaphore()
    for d in range(1, ntp):
        signal(barrier, (sp, lax.rem(tp + d, ntp)))
    for d in (1, nsp - 1):
        signal(barrier, (lax.rem(sp + d, nsp), tp))
    for d in range(1, NX):
        signal(barrier, (at_sp(0, d, cpos), tp))
    for d in (1, -1, 2, -2):
        signal(barrier, (at_sp(d, 0, cpos), tp))
    signal(barrier, (at_sp(0, 0, 1 - cpos), tp))
    greeted = ntp - 1 + 2 + NX - 1 + 4 + 1

    pairs = (
        (rt_h, rt),
        (doc_h, doc),
        (rw_h, rw),
        (ci_h, ci),
        (ig_h, ig),
        (og_h, og),
        (taps_h, taps),
        (fg_h, gains.at[tp]),
        (mg_h, mg),
        (ow_h, ow),
        (res_h, res),
        (wg_h.at[0], wg),
        (wu_h.at[0], wu),
        (wd_h.at[0], wd),
    )
    loads = [
        pltpu.make_async_copy(src, dst, load_sem.at[i]) for i, (src, dst) in enumerate(pairs)
    ]
    for load in loads:
        load.start()

    for i in range(3):
        loads[i].wait()
    experts_iota = lax.broadcasted_iota(jnp.int32, (nsp, tokens), 0)
    first = (experts_iota == rt[0:1, :]).astype(F32)
    second = (experts_iota == rt[1:2, :]).astype(F32)
    named = (first + second).astype(BF16)
    before = (
        lax.broadcasted_iota(jnp.int32, (tokens, tokens), 0)
        < lax.broadcasted_iota(jnp.int32, (tokens, tokens), 1)
    ).astype(F32).astype(BF16)
    earlier = jnp.dot(named, before, preferred_element_type=F32)
    slots = earlier + (experts_iota * cap).astype(F32)
    rows8[0:1, :] = doc[...].astype(F32)
    rows8[1:2, :] = jnp.sum(first * slots, axis=0, keepdims=True)
    rows8[2:3, :] = jnp.sum(second * slots, axis=0, keepdims=True)
    rows8[3:5, :] = rw[...]
    rows8[5:8, :] = jnp.zeros((3, tokens), F32)
    cols8[...] = jnp.transpose(rows8[...])

    for i in range(3, 8):
        loads[i].wait()
    value = (ig[...].astype(F32) * ci[...].astype(F32)).astype(BF16).astype(F32)
    joined[8:, :] = value
    docj[8:, :] = jnp.broadcast_to(cols8[:, 0:1], (tokens, channels))
    halo_out[0:8, :] = value[tokens - 8 :, :]
    halo_out[8:16, :] = jnp.broadcast_to(cols8[tokens - 8 :, 0:1], (8, channels))

    def convolve(lo, hi):
        docs_now = docj[8 + lo : 8 + hi, :]
        same_one = (docj[7 + lo : 7 + hi, :] == docs_now).astype(F32)
        same_two = (docj[6 + lo : 6 + hi, :] == docs_now).astype(F32)
        conv_sum = (
            taps[2:3, :] * joined[8 + lo : 8 + hi, :]
            + taps[1:2, :] * joined[7 + lo : 7 + hi, :] * same_one
            + taps[0:1, :] * joined[6 + lo : 6 + hi, :] * same_two
        )
        mix[tp, lo:hi, :] = (og[lo:hi, :].astype(F32) * conv_sum).astype(BF16)

    def to_tp(ref, send, recv):
        copies = []
        for d in (2, 1, ntp - 1):
            copies.append(
                pltpu.make_async_remote_copy(
                    src_ref=ref,
                    dst_ref=ref,
                    send_sem=send.at[d - 1],
                    recv_sem=recv.at[d - 1],
                    device_id=(sp, lax.rem(tp + d, ntp)),
                    device_id_type=MESH,
                )
            )
        for copy in copies:
            copy.start()
        return copies

    edge = 16
    convolve(edge, tokens)
    with jax.named_scope("barrier"):
        pl.semaphore_wait(barrier, greeted)
    halo = pltpu.make_async_remote_copy(
        src_ref=halo_out,
        dst_ref=halo_in,
        send_sem=halo_sem.at[0],
        recv_sem=halo_sem.at[1],
        device_id=(lax.rem(sp + 1, nsp), tp),
        device_id_type=MESH,
    )
    halo.start()
    for d in (2, -2):
        signal(round_sem.at[0], (at_sp(d, 0, cpos), tp))
    copies = to_tp(mix.at[tp, pl.ds(edge, tokens - edge)], mix_s.at[0], mix_r.at[0])
    copies += to_tp(gains.at[tp], gain_s, gain_r)

    line = lax.broadcasted_iota(jnp.int32, (region, tokens), 0)
    for r, dz in enumerate(OFFSETS):
        slot = (line + lax.rem(zpos + (dz + nz), nz) * region).astype(F32)
        hit = (slot == rows8[1:2, :]) | (slot == rows8[2:3, :])
        perm[r] = hit.astype(F32).astype(BF16)

    with jax.named_scope("halowait"):
        halo.wait()
    joined[0:8, :] = halo_in[0:8, :]
    docj[0:8, :] = jnp.where(sp == 0, -1.0, halo_in[8:16, :])
    convolve(0, edge)
    copies += to_tp(mix.at[tp, pl.ds(0, edge)], mix_s.at[1], mix_r.at[1])
    pl.semaphore_wait(round_sem.at[0], 2)
    for d in range(1, NX):
        signal(round_sem.at[1], (at_sp(0, d, cpos), tp))

    for i in range(8, 11):
        loads[i].wait()
    with jax.named_scope("mixwait"):
        for copy in copies:
            copy.wait()
    pl.semaphore_wait(round_sem.at[1], NX - 1)
    signal(round_sem.at[2], (at_sp(0, 0, 1 - cpos), tp))
    pieces = jnp.concatenate([mix[q] for q in range(ntp)], axis=1).astype(F32)
    squares = jnp.sum(pieces * pieces, axis=1, keepdims=True)
    mix_scale = lax.rsqrt(squares / (channels * ntp) + EPS)
    scaled = (pieces * mg[...]).astype(BF16)
    projected = jnp.dot(scaled, ow[...], preferred_element_type=F32)
    hidden = res[...].astype(F32) + projected * mix_scale
    hid[...] = hidden
    gained = (hidden * gains[tp]).astype(BF16)
    tok[tp] = gained

    def tp_copy(src, dst, send, recv, to):
        return pltpu.make_async_remote_copy(
            src_ref=src,
            dst_ref=dst,
            send_sem=send,
            recv_sem=recv,
            device_id=(sp, to),
            device_id_type=MESH,
        )

    def got(ref, sem):
        with jax.named_scope("wait"):
            pltpu.make_async_copy(ref, ref, sem).wait()

    def ring_own(buffer, start, rows, k):
        half = rows // 2
        upper = buffer.at[tp, pl.ds(start, half)]
        lower = buffer.at[tp, pl.ds(start + half, half)]
        tp_copy(upper, upper, ag_s.at[0, k], ag_r.at[0, k], right).start()
        tp_copy(lower, lower, ag_s.at[1, k], ag_r.at[1, k], left).start()
        tp_copy(lower, lower, ag_s.at[2, k], ag_r.at[2, k], right).start()
        tp_copy(upper, upper, ag_s.at[3, k], ag_r.at[3, k], left).start()

    def ring_forward(buffer, start, rows, k):
        half = rows // 2
        upper = buffer.at[left, pl.ds(start, half)]
        lower = buffer.at[right, pl.ds(start + half, half)]
        got(upper, ag_r.at[0, k])
        tp_copy(upper, upper, ag_s.at[4, k], ag_r.at[4, k], right).start()
        got(lower, ag_r.at[1, k])
        tp_copy(lower, lower, ag_s.at[5, k], ag_r.at[5, k], left).start()

    def ring_rest(buffer, start, rows, k):
        half = rows // 2
        got(buffer.at[left, pl.ds(start + half, half)], ag_r.at[2, k])
        got(buffer.at[right, pl.ds(start, half)], ag_r.at[3, k])
        got(buffer.at[opposite, pl.ds(start, half)], ag_r.at[4, k])
        got(buffer.at[opposite, pl.ds(start + half, half)], ag_r.at[5, k])

    tokens_piece = len(PIECES)
    ring_own(tok, 0, tokens, tokens_piece)
    with jax.named_scope("roundwait"):
        pl.semaphore_wait(round_sem.at[2], 1)

    mine = xpos * CORES + cpos
    my_rows = pl.multiple_of(mine * cap, cap)

    def exchange(src, dst, send, recv, r, dz):
        zz = lax.rem(zpos + (dz + nz), nz)

        def one(i, carry):
            to = lax.rem(mine + i, peers)
            pltpu.make_async_remote_copy(
                src_ref=src(r, pl.multiple_of(to * cap, cap)),
                dst_ref=dst(r, my_rows),
                send_sem=send.at[r],
                recv_sem=recv.at[r],
                device_id=(zz * peers + to, tp),
                device_id_type=MESH,
            ).start()
            return carry

        lax.fori_loop(1 if r == 0 else 0, peers, one, 0)

    def rows_of(r):
        return region - cap if r == 0 else region

    for r in range(NEAR, len(OFFSETS)):
        outgo[r - NEAR] = jnp.dot(perm[r], gained, preferred_element_type=F32).astype(BF16)
        exchange(
            lambda r, at: outgo.at[r - NEAR, pl.ds(at, cap)],
            lambda r, at: xin.at[tp, pl.ds(r * region + at, cap)],
            disp_s,
            disp_r,
            r,
            OFFSETS[r],
        )

    def near():
        ring_rest(tok, 0, tokens, tokens_piece)
        for r in range(NEAR):
            for q in range(ntp):
                outrow[q, r * region : (r + 1) * region, :] = jnp.dot(
                    perm[r], tok[q], preferred_element_type=F32
                ).astype(BF16)
            if r == 0:
                for q in range(ntp):
                    xin[q, pl.ds(my_rows, cap), :] = outrow[q, pl.ds(my_rows, cap), :]
            exchange(
                lambda r, at: outrow.at[:, pl.ds(r * region + at, cap)],
                lambda r, at: xin.at[:, pl.ds(r * region + at, cap)],
                disp_s,
                disp_r,
                r,
                OFFSETS[r],
            )

    def arrived(k):
        first_region, count = PIECES[k]
        for r in range(first_region, first_region + count):
            if r < NEAR:
                got(xin.at[:, pl.ds(r * region, rows_of(r))], disp_r.at[r])
            else:
                got(xin.at[tp, pl.ds(r * region, region)], disp_r.at[r])

    def span(k):
        return PIECES[k][0] * region, PIECES[k][1] * region

    def own(k):
        arrived(k)
        ring_own(xin, *span(k), k)

    def forward(k):
        ring_forward(xin, *span(k), k)

    width = features * ntp
    hidden_units = wg.shape[1]
    tile = 128
    wide = 256

    def experts_up(start, rows):
        total = jnp.zeros((rows, tile), F32)
        for q in range(ntp):
            weight = 1.0 / (gains[q] * gains[q])
            for c in range(features // tile):
                cut = slice(c * tile, (c + 1) * tile)
                x = xin[q, start : start + rows, cut].astype(F32)
                total = total + x * x * weight[:, cut]
        scale = lax.rsqrt(jnp.sum(total, axis=1, keepdims=True) / width + EPS)
        scl[0:rows, :] = jnp.broadcast_to(scale, (rows, tile))

        def up_tile(n, carry):
            at = pl.ds(pl.multiple_of(n * tile, tile), tile)
            x = jnp.concatenate([xin[q, start : start + rows] for q in range(ntp)], axis=1)
            both = jnp.concatenate([wg[:, at], wu[:, at]], axis=1)
            made = jnp.dot(x, both, preferred_element_type=F32)
            gate = made[:, :tile] * scl[0:rows, :]
            act[0:rows, at] = (
                jax.nn.silu(gate) * (made[:, tile:] * scl[0:rows, :])
            ).astype(BF16)
            return carry

        lax.fori_loop(0, hidden_units // tile, up_tile, 0)

    def experts_down(start, rows):
        for q in range(ntp):
            for k in range(features // wide):
                cols = slice(q * features + k * wide, q * features + (k + 1) * wide)
                part[q, start : start + rows, k * wide : (k + 1) * wide] = jnp.dot(
                    act[0:rows, :], wd[:, cols], preferred_element_type=F32
                ).astype(BF16)

    def reduce_start(k):
        start, rows = span(k)
        half = rows // 2
        upper = pl.ds(start, half)
        lower = pl.ds(start + half, half)
        tp_copy(part.at[opposite, upper], rx.at[upper], rs_s.at[0, k], rs_r.at[0, k], right).start()
        tp_copy(part.at[opposite, lower], rx.at[lower], rs_s.at[1, k], rs_r.at[1, k], left).start()
        tp_copy(part.at[right, lower], fl.at[lower], rs_s.at[2, k], rs_r.at[2, k], right).start()
        tp_copy(part.at[left, upper], fr.at[upper], rs_s.at[3, k], rs_r.at[3, k], left).start()

    def reduce_add(k):
        start, rows = span(k)
        half = rows // 2
        upper = pl.ds(start, half)
        lower = pl.ds(start + half, half)
        got(rx.at[upper], rs_r.at[0, k])
        part[right, upper, :] = (
            part[right, upper, :].astype(F32) + rx[upper, :].astype(F32)
        ).astype(BF16)
        tp_copy(part.at[right, upper], fl.at[upper], rs_s.at[4, k], rs_r.at[4, k], right).start()
        got(rx.at[lower], rs_r.at[1, k])
        part[left, lower, :] = (
            part[left, lower, :].astype(F32) + rx[lower, :].astype(F32)
        ).astype(BF16)
        tp_copy(part.at[left, lower], fr.at[lower], rs_s.at[5, k], rs_r.at[5, k], left).start()

    def give_back(k):
        start, rows = span(k)
        half = rows // 2
        upper = pl.ds(start, half)
        lower = pl.ds(start + half, half)
        got(fl.at[lower], rs_r.at[2, k])
        got(fr.at[upper], rs_r.at[3, k])
        got(fl.at[upper], rs_r.at[4, k])
        got(fr.at[lower], rs_r.at[5, k])
        whole = pl.ds(start, rows)
        ret[whole, :] = (
            part[tp, whole, :].astype(F32) + fl[whole, :].astype(F32) + fr[whole, :].astype(F32)
        ).astype(BF16)
        first_region, count = PIECES[k]
        for r in range(first_region, first_region + count):
            if r == 0:
                ret_in[pl.ds(my_rows, cap), :] = ret[pl.ds(my_rows, cap), :]
            exchange(
                lambda r, at: ret.at[pl.ds(r * region + at, cap)],
                lambda r, at: ret_in.at[pl.ds(r * region + at, cap)],
                ret_s,
                ret_r,
                r,
                -OFFSETS[r],
            )

    lane = lax.broadcasted_iota(jnp.int32, (tokens, region), 1)

    def combine(k):
        first_region, count = PIECES[k]
        for r in range(first_region, first_region + count):
            got(ret_in.at[pl.ds(r * region, rows_of(r))], ret_r.at[r])
        start, rows = span(k)
        picks = [[], []]
        for r in range(first_region, first_region + count):
            slot = (lane + lax.rem(zpos + (OFFSETS[r] + nz), nz) * region).astype(F32)
            for i in range(2):
                picks[i].append((slot == cols8[:, 1 + i : 2 + i]).astype(F32).astype(BF16))
        routed = hid[...]
        for i in range(2):
            pick = jnp.concatenate(picks[i], axis=1)
            routed = routed + cols8[:, 3 + i : 4 + i] * jnp.dot(
                pick, ret_in[start : start + rows, :], preferred_element_type=F32
            )
        hid[...] = routed

    def gone(ref, sem):
        pltpu.make_async_copy(ref, ref, sem).wait()

    def all_gone():
        for r in range(len(OFFSETS)):
            if r < NEAR:
                gone(outrow.at[:, pl.ds(0, rows_of(r))], disp_s.at[r])
            else:
                gone(outgo.at[r - NEAR], disp_s.at[r])
            gone(ret.at[pl.ds(0, rows_of(r))], ret_s.at[r])
        for k in range(len(PIECES)):
            half = span(k)[1] // 2
            for i in range(6):
                if k < 3:
                    gone(xin.at[tp, pl.ds(0, half)], ag_s.at[i, k])
                gone(part.at[0, pl.ds(0, half)], rs_s.at[i, k])
        for i in range(6):
            gone(tok.at[tp, pl.ds(0, tokens // 2)], ag_s.at[i, tokens_piece])

    steps = {
        "own": own,
        "forward": forward,
        "up": lambda k: (ring_rest(xin, *span(k), k), experts_up(*span(k))),
        "down": lambda k: experts_down(*span(k)),
        "add": reduce_add,
        "back": give_back,
        "combine": combine,
        "tokens": lambda k: ring_forward(tok, 0, tokens, tokens_piece),
        "near": lambda k: near(),
        "weights": lambda k: [loads[i].wait() for i in range(11, 14)],
        "upz": lambda k: (arrived(4), experts_up(*span(4))),
        "downz": lambda k: experts_down(*span(4)),
        "upn": lambda k: (arrived(3), experts_up(*span(3))),
        "downn": lambda k: experts_down(*span(3)),
        "start": reduce_start,
        "gone": lambda k: all_gone(),
    }
    for name, k in ORDER:
        with jax.named_scope(f"{name}{k}"):
            steps[name](k)
    with jax.named_scope("out"):
        out_ref[...] = hid[...].astype(BF16)

def per_device(
    residual_in,
    conv_input,
    outer_gate,
    inner_gate,
    documents,
    conv_taps,
    mixer_gain,
    output_weight,
    ffn_gain,
    routes,
    route_weights,
    expert_gate,
    expert_up,
    expert_down,
):
    nsp = lax.axis_size("sp")
    ntp = lax.axis_size("tp")
    tokens, features = residual_in.shape
    channels = conv_input.shape[1]
    cap = 4 * tokens // nsp
    region = NX * CORES * cap
    slots = nsp * cap
    width = features * ntp
    hidden_units = expert_gate.shape[2]
    args = (
        residual_in,
        conv_input,
        outer_gate,
        inner_gate,
        documents.reshape(1, tokens),
        conv_taps,
        mixer_gain.reshape(1, -1),
        output_weight,
        ffn_gain.reshape(1, -1),
        routes.T,
        route_weights.T,
        expert_gate,
        expert_up,
        expert_down,
    )
    locals_ = [
        pltpu.VMEM(a.shape if a.ndim == 2 else a.shape[1:], a.dtype) for a in args
    ]
    dma = pltpu.SemaphoreType.DMA
    scratch = locals_ + [
        pltpu.VMEM((8, tokens), F32),
        pltpu.VMEM((tokens, 8), F32),
        pltpu.VMEM((tokens + 8, channels), F32),
        pltpu.VMEM((tokens + 8, channels), F32),
        pltpu.VMEM((16, channels), F32),
        pltpu.VMEM((16, channels), F32),
        pltpu.VMEM((ntp, 1, features), F32),
        pltpu.VMEM((ntp, tokens, channels), BF16),
        pltpu.VMEM((ntp, tokens, features), BF16),
        pltpu.VMEM((tokens, features), F32),
        pltpu.VMEM((len(OFFSETS), region, tokens), BF16),
        pltpu.VMEM((len(OFFSETS) - NEAR, region, features), BF16),
        pltpu.VMEM((ntp, NEAR * region, features), BF16),
        pltpu.VMEM((ntp, slots, features), BF16),
        pltpu.VMEM((NEAR * region, 128), F32),
        pltpu.VMEM((NEAR * region, hidden_units), BF16),
        pltpu.VMEM((ntp, slots, features), BF16),
        pltpu.VMEM((slots, features), BF16),
        pltpu.VMEM((slots, features), BF16),
        pltpu.VMEM((slots, features), BF16),
        pltpu.VMEM((slots, features), BF16),
        pltpu.VMEM((slots, features), BF16),
        dma((len(args),)),
        dma((2,)),
        dma((ntp - 1,)),
        dma((ntp - 1,)),
        dma((2, ntp - 1)),
        dma((2, ntp - 1)),
        dma((len(OFFSETS),)),
        dma((len(OFFSETS),)),
        dma((6, len(PIECES) + 1)),
        dma((6, len(PIECES) + 1)),
        dma((6, len(PIECES))),
        dma((6, len(PIECES))),
        dma((len(OFFSETS),)),
        dma((len(OFFSETS),)),
        pltpu.SemaphoreType.REGULAR((3,)),
    ]
    return pl.pallas_call(
        functools.partial(layer_kernel, nsp, ntp, cap),
        out_shape=jax.ShapeDtypeStruct((tokens, features), BF16),
        in_specs=[pl.BlockSpec(memory_space=pl.ANY)] * len(args),
        out_specs=pl.BlockSpec(memory_space=pltpu.VMEM),
        scratch_shapes=scratch,
        compiler_params=pltpu.CompilerParams(
            collective_id=0, has_side_effects=True, vmem_limit_bytes=60 * 1024 * 1024
        ),
        cost_estimate=pl.CostEstimate(
            flops=6 * nsp * cap * width * hidden_units,
            bytes_accessed=6 * width * hidden_units,
            transcendentals=0,
        ),
        name="layer",
    )(*args)


def solution(mesh):
    placed = (
        P("sp", "tp"),
        P("sp", "tp"),
        P("sp", "tp"),
        P("sp", "tp"),
        P("sp"),
        P(None, "tp"),
        P(),
        P(None, "tp"),
        P("tp"),
        P("sp", None),
        P("sp", None),
        P("sp", None, "tp"),
        P("sp", None, "tp"),
        P("sp", "tp", None),
    )
    return jax.shard_map(
        per_device, mesh=mesh, in_specs=placed, out_specs=P("sp", "tp"), check_vma=False
    )
```

time: 117 us -> 97.2 us (0.83)
  Pallas kernels: 115 us -> 95.4 us
    pallas_call x1, Pallas kernels: 115 us -> 95.4 us  [per_device(): pl.pallas_call(functools.partial(layer_kernel, nsp, ntp, cap), out_shape=...]
where the time goes in v2:
time: 97.2 us; the launch traced here: 97.1 us
  Pallas kernels  95.4 us (98%)
  local copies, waits for them, and re-layouts  1.67 us (2%)
    pallas_call x1, Pallas kernels, per_device(): pl.pallas_call(functools.partial(layer_kernel, nsp, ntp, cap), out_shape=...  95.4 us

profile of v2, /device:TPU:1, one launch (start us, length us, event | category | flops | bytes accessed | tf_op | source)
XLA Modules:
  0.0 97.1 jit_solution(697343437255526676)
XLA Ops:
  0.0 95.4 %layer.1 = bf16[256,512]{1,0:T(8,128)(2,1)} custom-call(bf16[256,512]{1,0:T(8,128)(2,1)} %res_h.1, bf16[256,128]{1,0:T(8,128)(2,1)} %ci_h.1, bf16[256,128]{1,0:T(8,128)(2,1)} %og_h.1, bf16[256,128]{1,0:T(8,128)(2,1)} %ig_h.1, s32[1,256]{1,0:T(1,128)} %bitcast.9, f32[3,128]{1,0:T(4,128)} %taps_h.1, f32[1,512]{1,0:T(1,128)} %bitcast.5, bf16[512,512]{1,0:T(8,128)(2,1)} %ow_h.1, ...), custom_call_target="tpu_custom_call" | custom-call | flops 11274289152 | bytes 11010048 | tf_op jit(solution)/shard_map/layer/pallas_call | solution.py:647
  95.4 1.7 %copy.16 = bf16[256,512]{1,0:T(8,128)(2,1)} copy(bf16[256,512]{1,0:T(8,128)(2,1)} %layer.1) | data formatting | bytes 524288

commit v3 on v2

--- a/solution.py
+++ b/solution.py
@@ -10,45 +10,69 @@
 EPS = 1e-06
 CORES = 2
 NX = 4
-OFFSETS = (0, 1, -1, 2, -2, 3, -3, 4)
+REGIONS = (
+    (0, 0, 8),
+    (1, 0, 8),
+    (-1, 0, 8),
+    (2, 0, 4),
+    (-2, 0, 4),
+    (2, 4, 4),
+    (-2, 4, 4),
+    (3, 0, 4),
+    (-3, 0, 4),
+    (3, 4, 4),
+    (-3, 4, 4),
+    (4, 0, 8),
+)
 NEAR = 3
-PIECES = ((3, 2), (5, 2), (7, 1), (1, 2), (0, 1))
+RINGS = ((3, 4), (5, 6), (7, 8), (9, 10), (11,))
+RING = len(RINGS)
+PIECES = ((3, 4, 5, 6), (7, 8, 9, 10), (11,), (1, 2), (0,))
 ORDER = (
     ("tokens", 0),
     ("own", 0),
     ("near", 0),
+    ("own", 1),
     ("forward", 0),
+    ("own", 2),
+    ("forward", 1),
+    ("forward", 2),
+    ("own", 3),
     ("weights", 0),
-    ("own", 1),
+    ("rest", 0),
+    ("rest", 1),
     ("up", 0),
-    ("forward", 1),
+    ("forward", 3),
     ("down", 0),
-    ("own", 2),
+    ("own", 4),
     ("start", 0),
-    ("upz", 0),
-    ("downz", 0),
+    ("up", 4),
+    ("down", 4),
+    ("rest", 2),
+    ("rest", 3),
     ("up", 1),
-    ("forward", 2),
+    ("forward", 4),
     ("down", 1),
     ("add", 0),
     ("start", 1),
+    ("up", 3),
+    ("down", 3),
+    ("back", 0),
+    ("rest", 4),
     ("up", 2),
+    ("add", 1),
     ("down", 2),
     ("start", 2),
-    ("back", 0),
-    ("upn", 0),
-    ("add", 1),
-    ("downn", 0),
+    ("start", 4),
+    ("back", 1),
     ("add", 2),
     ("start", 3),
-    ("start", 4),
-    ("back", 1),
+    ("add", 4),
     ("back", 2),
+    ("combine", 0),
     ("add", 3),
-    ("add", 4),
-    ("combine", 0),
+    ("back", 4),
     ("back", 3),
-    ("back", 4),
     ("combine", 1),
     ("combine", 2),
     ("gone", 0),
@@ -117,8 +141,6 @@
     ret_in,
     load_sem,
     halo_sem,
-    gain_s,
-    gain_r,
     mix_s,
     mix_r,
     disp_s,
@@ -140,7 +162,13 @@
     tokens, features = res.shape
     channels = ci.shape[1]
     peers = NX * CORES
-    region = peers * cap
+    plane = peers * cap
+    mine = xpos * CORES + cpos
+    base, most = [], 0
+    for _, _, count in REGIONS:
+        base.append(most)
+        most += count * cap
+    sizes = [count * cap for _, _, count in REGIONS]
     left = lax.rem(tp + ntp - 1, ntp)
     right = lax.rem(tp + 1, ntp)
     opposite = lax.rem(tp + 2, ntp)
@@ -226,21 +254,19 @@
         mix[tp, lo:hi, :] = (og[lo:hi, :].astype(F32) * conv_sum).astype(BF16)
 
     def to_tp(ref, send, recv):
-        copies = []
         for d in (2, 1, ntp - 1):
-            copies.append(
-                pltpu.make_async_remote_copy(
-                    src_ref=ref,
-                    dst_ref=ref,
-                    send_sem=send.at[d - 1],
-                    recv_sem=recv.at[d - 1],
-                    device_id=(sp, lax.rem(tp + d, ntp)),
-                    device_id_type=MESH,
-                )
-            )
-        for copy in copies:
-            copy.start()
-        return copies
+            pltpu.make_async_remote_copy(
+                src_ref=ref,
+                dst_ref=ref,
+                send_sem=send,
+                recv_sem=recv,
+                device_id=(sp, lax.rem(tp + d, ntp)),
+                device_id_type=MESH,
+            ).start()
+
+    def got(ref, sem):
+        with jax.named_scope("wait"):
+            pltpu.make_async_copy(ref, ref, sem).wait()
 
     edge = 16
     convolve(edge, tokens)
@@ -257,21 +283,27 @@
     halo.start()
     for d in (2, -2):
         signal(round_sem.at[0], (at_sp(d, 0, cpos), tp))
-    copies = to_tp(mix.at[tp, pl.ds(edge, tokens - edge)], mix_s.at[0], mix_r.at[0])
-    copies += to_tp(gains.at[tp], gain_s, gain_r)
-
-    line = lax.broadcasted_iota(jnp.int32, (region, tokens), 0)
-    for r, dz in enumerate(OFFSETS):
-        slot = (line + lax.rem(zpos + (dz + nz), nz) * region).astype(F32)
+    to_tp(mix.at[tp, pl.ds(edge, tokens - edge)], mix_s.at[0], mix_r.at[0])
+    to_tp(gains.at[tp], mix_s.at[1], mix_r.at[1])
+
+    def slots_of(r, shape, dim):
+        dz, skip, _ = REGIONS[r]
+        line = lax.broadcasted_iota(jnp.int32, shape, dim)
+        peer = lax.rem(line // cap + (mine + skip), peers)
+        zz = lax.rem(zpos + (dz + nz), nz)
+        return (zz * plane + peer * cap + lax.rem(line, cap)).astype(F32)
+
+    for r in range(len(REGIONS)):
+        slot = slots_of(r, (sizes[r], tokens), 0)
         hit = (slot == rows8[1:2, :]) | (slot == rows8[2:3, :])
-        perm[r] = hit.astype(F32).astype(BF16)
+        perm[base[r] : base[r] + sizes[r], :] = hit.astype(F32).astype(BF16)
 
     with jax.named_scope("halowait"):
         halo.wait()
     joined[0:8, :] = halo_in[0:8, :]
     docj[0:8, :] = jnp.where(sp == 0, -1.0, halo_in[8:16, :])
     convolve(0, edge)
-    copies += to_tp(mix.at[tp, pl.ds(0, edge)], mix_s.at[1], mix_r.at[1])
+    to_tp(mix.at[tp, pl.ds(0, edge)], mix_s.at[0], mix_r.at[0])
     pl.semaphore_wait(round_sem.at[0], 2)
     for d in range(1, NX):
         signal(round_sem.at[1], (at_sp(0, d, cpos), tp))
@@ -279,8 +311,8 @@
     for i in range(8, 11):
         loads[i].wait()
     with jax.named_scope("mixwait"):
-        for copy in copies:
-            copy.wait()
+        got(mix.at[pl.ds(0, ntp - 1)], mix_r.at[0])
+        got(gains.at[pl.ds(0, ntp - 1)], mix_r.at[1])
     pl.semaphore_wait(round_sem.at[1], NX - 1)
     signal(round_sem.at[2], (at_sp(0, 0, 1 - cpos), tp))
     pieces = jnp.concatenate([mix[q] for q in range(ntp)], axis=1).astype(F32)
@@ -303,110 +335,111 @@
             device_id_type=MESH,
         )
 
-    def got(ref, sem):
-        with jax.named_scope("wait"):
-            pltpu.make_async_copy(ref, ref, sem).wait()
-
     def ring_own(buffer, start, rows, k):
         half = rows // 2
         upper = buffer.at[tp, pl.ds(start, half)]
         lower = buffer.at[tp, pl.ds(start + half, half)]
-        tp_copy(upper, upper, ag_s.at[0, k], ag_r.at[0, k], right).start()
-        tp_copy(lower, lower, ag_s.at[1, k], ag_r.at[1, k], left).start()
-        tp_copy(lower, lower, ag_s.at[2, k], ag_r.at[2, k], right).start()
-        tp_copy(upper, upper, ag_s.at[3, k], ag_r.at[3, k], left).start()
+        tp_copy(upper, upper, ag_s.at[0], ag_r.at[0, k], right).start()
+        tp_copy(lower, lower, ag_s.at[0], ag_r.at[1, k], left).start()
+        tp_copy(lower, lower, ag_s.at[0], ag_r.at[2, k], right).start()
+        tp_copy(upper, upper, ag_s.at[0], ag_r.at[2, k], left).start()
 
     def ring_forward(buffer, start, rows, k):
         half = rows // 2
         upper = buffer.at[left, pl.ds(start, half)]
         lower = buffer.at[right, pl.ds(start + half, half)]
         got(upper, ag_r.at[0, k])
-        tp_copy(upper, upper, ag_s.at[4, k], ag_r.at[4, k], right).start()
+        tp_copy(upper, upper, ag_s.at[0], ag_r.at[2, k], right).start()
         got(lower, ag_r.at[1, k])
-        tp_copy(lower, lower, ag_s.at[5, k], ag_r.at[5, k], left).start()
+        tp_copy(lower, lower, ag_s.at[0], ag_r.at[2, k], left).start()
 
     def ring_rest(buffer, start, rows, k):
-        half = rows // 2
-        got(buffer.at[left, pl.ds(start + half, half)], ag_r.at[2, k])
-        got(buffer.at[right, pl.ds(start, half)], ag_r.at[3, k])
-        got(buffer.at[opposite, pl.ds(start, half)], ag_r.at[4, k])
-        got(buffer.at[opposite, pl.ds(start + half, half)], ag_r.at[5, k])
-
-    tokens_piece = len(PIECES)
-    ring_own(tok, 0, tokens, tokens_piece)
+        got(buffer.at[pl.ds(0, 2), pl.ds(start, rows)], ag_r.at[2, k])
+
+    ring_own(tok, 0, tokens, RING)
     with jax.named_scope("roundwait"):
         pl.semaphore_wait(round_sem.at[2], 1)
 
-    mine = xpos * CORES + cpos
-    my_rows = pl.multiple_of(mine * cap, cap)
-
-    def exchange(src, dst, send, recv, r, dz):
-        zz = lax.rem(zpos + (dz + nz), nz)
+    def exchange(src, dst, send, recv, r, way):
+        dz, skip, count = REGIONS[r]
+        zz = lax.rem(zpos + (way * dz + nz), nz)
 
         def one(i, carry):
-            to = lax.rem(mine + i, peers)
+            at = pl.ds(pl.multiple_of(base[r] + i * cap, cap), cap)
+            to = lax.rem(mine + way * (i + skip) + peers, peers)
             pltpu.make_async_remote_copy(
-                src_ref=src(r, pl.multiple_of(to * cap, cap)),
-                dst_ref=dst(r, my_rows),
-                send_sem=send.at[r],
-                recv_sem=recv.at[r],
+                src_ref=src(at),
+                dst_ref=dst(at),
+                send_sem=send,
+                recv_sem=recv,
                 device_id=(zz * peers + to, tp),
                 device_id_type=MESH,
             ).start()
             return carry
 
-        lax.fori_loop(1 if r == 0 else 0, peers, one, 0)
-
-    def rows_of(r):
-        return region - cap if r == 0 else region
-
-    for r in range(NEAR, len(OFFSETS)):
-        outgo[r - NEAR] = jnp.dot(perm[r], gained, preferred_element_type=F32).astype(BF16)
+        lax.fori_loop(1 if r == 0 else 0, count, one, 0)
+
+    ring_of = {r: g for g, regions in enumerate(RINGS) for r in regions}
+
+    def extent(regions):
+        return base[regions[0]], sum(sizes[r] for r in regions)
+
+    def crossed(regions):
+        start, rows = extent(regions)
+        skip = cap if 0 in regions else 0
+        return pl.ds(start + skip, rows - skip)
+
+    def rows_at(r):
+        return slice(base[r], base[r] + sizes[r])
+
+    for r in range(NEAR, len(REGIONS)):
+        outgo[rows_at(r), :] = jnp.dot(
+            perm[rows_at(r), :], gained, preferred_element_type=F32
+        ).astype(BF16)
         exchange(
-            lambda r, at: outgo.at[r - NEAR, pl.ds(at, cap)],
-            lambda r, at: xin.at[tp, pl.ds(r * region + at, cap)],
-            disp_s,
-            disp_r,
+            lambda at: outgo.at[at],
+            lambda at: xin.at[tp, at],
+            disp_s.at[0],
+            disp_r.at[ring_of[r]],
             r,
-            OFFSETS[r],
+            1,
         )
 
     def near():
-        ring_rest(tok, 0, tokens, tokens_piece)
+        ring_rest(tok, 0, tokens, RING)
         for r in range(NEAR):
             for q in range(ntp):
-                outrow[q, r * region : (r + 1) * region, :] = jnp.dot(
-                    perm[r], tok[q], preferred_element_type=F32
+                outrow[q, rows_at(r), :] = jnp.dot(
+                    perm[rows_at(r), :], tok[q], preferred_element_type=F32
                 ).astype(BF16)
             if r == 0:
                 for q in range(ntp):
-                    xin[q, pl.ds(my_rows, cap), :] = outrow[q, pl.ds(my_rows, cap), :]
+                    xin[q, 0:cap, :] = outrow[q, 0:cap, :]
             exchange(
-                lambda r, at: outrow.at[:, pl.ds(r * region + at, cap)],
-                lambda r, at: xin.at[:, pl.ds(r * region + at, cap)],
-                disp_s,
-                disp_r,
+                lambda at: outrow.at[:, at],
+                lambda at: xin.at[:, at],
+                disp_s.at[1],
+                disp_r.at[RING + min(r, 1)],
                 r,
-                OFFSETS[r],
+                1,
             )
 
+    def span(k):
+        return extent(PIECES[k])
+
     def arrived(k):
-        first_region, count = PIECES[k]
-        for r in range(first_region, first_region + count):
-            if r < NEAR:
-                got(xin.at[:, pl.ds(r * region, rows_of(r))], disp_r.at[r])
-            else:
-                got(xin.at[tp, pl.ds(r * region, region)], disp_r.at[r])
-
-    def span(k):
-        return PIECES[k][0] * region, PIECES[k][1] * region
-
-    def own(k):
-        arrived(k)
-        ring_own(xin, *span(k), k)
-
-    def forward(k):
-        ring_forward(xin, *span(k), k)
+        if PIECES[k][0] < NEAR:
+            got(xin.at[:, crossed(PIECES[k])], disp_r.at[RING + min(PIECES[k][0], 1)])
+
+    def own(g):
+        got(xin.at[tp, crossed(RINGS[g])], disp_r.at[g])
+        ring_own(xin, *extent(RINGS[g]), g)
+
+    def forward(g):
+        ring_forward(xin, *extent(RINGS[g]), g)
+
+    def rest(g):
+        ring_rest(xin, *extent(RINGS[g]), g)
 
     width = features * ntp
     hidden_units = wg.shape[1]
@@ -450,10 +483,10 @@
         half = rows // 2
         upper = pl.ds(start, half)
         lower = pl.ds(start + half, half)
-        tp_copy(part.at[opposite, upper], rx.at[upper], rs_s.at[0, k], rs_r.at[0, k], right).start()
-        tp_copy(part.at[opposite, lower], rx.at[lower], rs_s.at[1, k], rs_r.at[1, k], left).start()
-        tp_copy(part.at[right, lower], fl.at[lower], rs_s.at[2, k], rs_r.at[2, k], right).start()
-        tp_copy(part.at[left, upper], fr.at[upper], rs_s.at[3, k], rs_r.at[3, k], left).start()
+        tp_copy(part.at[opposite, upper], rx.at[upper], rs_s.at[0], rs_r.at[0, k], right).start()
+        tp_copy(part.at[opposite, lower], rx.at[lower], rs_s.at[0], rs_r.at[1, k], left).start()
+        tp_copy(part.at[right, lower], fl.at[lower], rs_s.at[0], rs_r.at[2, k], right).start()
+        tp_copy(part.at[left, upper], fr.at[upper], rs_s.at[0], rs_r.at[2, k], left).start()
 
     def reduce_add(k):
         start, rows = span(k)
@@ -464,93 +497,71 @@
         part[right, upper, :] = (
             part[right, upper, :].astype(F32) + rx[upper, :].astype(F32)
         ).astype(BF16)
-        tp_copy(part.at[right, upper], fl.at[upper], rs_s.at[4, k], rs_r.at[4, k], right).start()
+        tp_copy(part.at[right, upper], fl.at[upper], rs_s.at[0], rs_r.at[2, k], right).start()
         got(rx.at[lower], rs_r.at[1, k])
         part[left, lower, :] = (
             part[left, lower, :].astype(F32) + rx[lower, :].astype(F32)
         ).astype(BF16)
-        tp_copy(part.at[left, lower], fr.at[lower], rs_s.at[5, k], rs_r.at[5, k], left).start()
+        tp_copy(part.at[left, lower], fr.at[lower], rs_s.at[0], rs_r.at[2, k], left).start()
 
     def give_back(k):
         start, rows = span(k)
-        half = rows // 2
-        upper = pl.ds(start, half)
-        lower = pl.ds(start + half, half)
-        got(fl.at[lower], rs_r.at[2, k])
-        got(fr.at[upper], rs_r.at[3, k])
-        got(fl.at[upper], rs_r.at[4, k])
-        got(fr.at[lower], rs_r.at[5, k])
+        got(part.at[pl.ds(0, 2), pl.ds(start, rows)], rs_r.at[2, k])
         whole = pl.ds(start, rows)
         ret[whole, :] = (
             part[tp, whole, :].astype(F32) + fl[whole, :].astype(F32) + fr[whole, :].astype(F32)
         ).astype(BF16)
-        first_region, count = PIECES[k]
-        for r in range(first_region, first_region + count):
+        for r in PIECES[k]:
             if r == 0:
-                ret_in[pl.ds(my_rows, cap), :] = ret[pl.ds(my_rows, cap), :]
+                ret_in[0:cap, :] = ret[0:cap, :]
             exchange(
-                lambda r, at: ret.at[pl.ds(r * region + at, cap)],
-                lambda r, at: ret_in.at[pl.ds(r * region + at, cap)],
-                ret_s,
-                ret_r,
+                lambda at: ret.at[at],
+                lambda at: ret_in.at[at],
+                ret_s.at[0],
+                ret_r.at[k],
                 r,
-                -OFFSETS[r],
+                -1,
             )
 
-    lane = lax.broadcasted_iota(jnp.int32, (tokens, region), 1)
-
     def combine(k):
-        first_region, count = PIECES[k]
-        for r in range(first_region, first_region + count):
-            got(ret_in.at[pl.ds(r * region, rows_of(r))], ret_r.at[r])
+        got(ret_in.at[crossed(PIECES[k])], ret_r.at[k])
         start, rows = span(k)
         picks = [[], []]
-        for r in range(first_region, first_region + count):
-            slot = (lane + lax.rem(zpos + (OFFSETS[r] + nz), nz) * region).astype(F32)
+        for r in PIECES[k]:
+            slot = slots_of(r, (tokens, sizes[r]), 1)
             for i in range(2):
-                picks[i].append((slot == cols8[:, 1 + i : 2 + i]).astype(F32).astype(BF16))
+                picks[i].append((slot == cols8[:, 1 + i : 2 + i]).astype(F32))
         routed = hid[...]
         for i in range(2):
-            pick = jnp.concatenate(picks[i], axis=1)
+            pick = jnp.concatenate(picks[i], axis=1).astype(BF16)
             routed = routed + cols8[:, 3 + i : 4 + i] * jnp.dot(
                 pick, ret_in[start : start + rows, :], preferred_element_type=F32
             )
         hid[...] = routed
 
-    def gone(ref, sem):
-        pltpu.make_async_copy(ref, ref, sem).wait()
-
     def all_gone():
-        for r in range(len(OFFSETS)):
-            if r < NEAR:
-                gone(outrow.at[:, pl.ds(0, rows_of(r))], disp_s.at[r])
-            else:
-                gone(outgo.at[r - NEAR], disp_s.at[r])
-            gone(ret.at[pl.ds(0, rows_of(r))], ret_s.at[r])
-        for k in range(len(PIECES)):
-            half = span(k)[1] // 2
-            for i in range(6):
-                if k < 3:
-                    gone(xin.at[tp, pl.ds(0, half)], ag_s.at[i, k])
-                gone(part.at[0, pl.ds(0, half)], rs_s.at[i, k])
-        for i in range(6):
-            gone(tok.at[tp, pl.ds(0, tokens // 2)], ag_s.at[i, tokens_piece])
+        slots = xin.shape[1]
+        near_rows = sum(sizes[:NEAR])
+        got(mix.at[pl.ds(0, ntp - 1)], mix_s.at[0])
+        got(gains.at[pl.ds(0, ntp - 1)], mix_s.at[1])
+        got(outgo.at[pl.ds(near_rows, slots - near_rows)], disp_s.at[0])
+        got(outrow.at[:, pl.ds(cap, near_rows - cap)], disp_s.at[1])
+        got(ret.at[pl.ds(cap, slots - cap)], ret_s.at[0])
+        got(part.at[pl.ds(0, ntp - 1)], rs_s.at[0])
+        got(xin.at[pl.ds(0, ntp - 1), pl.ds(0, slots - near_rows + tokens)], ag_s.at[0])
 
     steps = {
         "own": own,
         "forward": forward,
-        "up": lambda k: (ring_rest(xin, *span(k), k), experts_up(*span(k))),
+        "rest": rest,
+        "up": lambda k: (arrived(k), experts_up(*span(k))),
         "down": lambda k: experts_down(*span(k)),
         "add": reduce_add,
         "back": give_back,
         "combine": combine,
-        "tokens": lambda k: ring_forward(tok, 0, tokens, tokens_piece),
+        "tokens": lambda k: ring_forward(tok, 0, tokens, RING),
         "near": lambda k: near(),
         "weights": lambda k: [loads[i].wait() for i in range(11, 14)],
-        "upz": lambda k: (arrived(4), experts_up(*span(4))),
-        "downz": lambda k: experts_down(*span(4)),
-        "upn": lambda k: (arrived(3), experts_up(*span(3))),
-        "downn": lambda k: experts_down(*span(3)),
         "start": reduce_start,
         "gone": lambda k: all_gone(),
     }
@@ -581,8 +592,9 @@
     tokens, features = residual_in.shape
     channels = conv_input.shape[1]
     cap = 4 * tokens // nsp
-    region = NX * CORES * cap
     slots = nsp * cap
+    sizes = [count * cap for _, _, count in REGIONS]
+    largest = max(sum(sizes[r] for r in piece) for piece in PIECES)
     width = features * ntp
     hidden_units = expert_gate.shape[2]
     args = (
@@ -616,12 +628,12 @@
         pltpu.VMEM((ntp, tokens, channels), BF16),
         pltpu.VMEM((ntp, tokens, features), BF16),
         pltpu.VMEM((tokens, features), F32),
-        pltpu.VMEM((len(OFFSETS), region, tokens), BF16),
-        pltpu.VMEM((len(OFFSETS) - NEAR, region, features), BF16),
-        pltpu.VMEM((ntp, NEAR * region, features), BF16),
+        pltpu.VMEM((slots, tokens), BF16),
+        pltpu.VMEM((slots, features), BF16),
+        pltpu.VMEM((ntp, sum(sizes[:NEAR]), features), BF16),
         pltpu.VMEM((ntp, slots, features), BF16),
-        pltpu.VMEM((NEAR * region, 128), F32),
-        pltpu.VMEM((NEAR * region, hidden_units), BF16),
+        pltpu.VMEM((largest, 128), F32),
+        pltpu.VMEM((largest, hidden_units), BF16),
         pltpu.VMEM((ntp, slots, features), BF16),
         pltpu.VMEM((slots, features), BF16),
         pltpu.VMEM((slots, features), BF16),
@@ -630,18 +642,16 @@
         pltpu.VMEM((slots, features), BF16),
         dma((len(args),)),
         dma((2,)),
-        dma((ntp - 1,)),
-        dma((ntp - 1,)),
-        dma((2, ntp - 1)),
-        dma((2, ntp - 1)),
-        dma((len(OFFSETS),)),
-        dma((len(OFFSETS),)),
-        dma((6, len(PIECES) + 1)),
-        dma((6, len(PIECES) + 1)),
-        dma((6, len(PIECES))),
-        dma((6, len(PIECES))),
-        dma((len(OFFSETS),)),
-        dma((len(OFFSETS),)),
+        dma((2,)),
+        dma((2,)),
+        dma((2,)),
+        dma((RING + 2,)),
+        dma((1,)),
+        dma((3, RING + 1)),
+        dma((1,)),
+        dma((3, len(PIECES))),
+        dma((1,)),
+        dma((len(PIECES),)),
         pltpu.SemaphoreType.REGULAR((3,)),
     ]
     return pl.pallas_call(

time: 97.2 us -> 94.8 us (0.975)
  Pallas kernels: 95.4 us -> 93 us
    pallas_call x1, Pallas kernels: 95.4 us -> 93 us  [per_device(): pl.pallas_call(functools.partial(layer_kernel, nsp, ntp, cap), out_shape=...]
where the time goes in v3:
time: 94.8 us; the launch traced here: 94.7 us
  Pallas kernels  93 us (98%)
  local copies, waits for them, and re-layouts  1.67 us (2%)
    pallas_call x1, Pallas kernels, per_device(): pl.pallas_call(functools.partial(layer_kernel, nsp, ntp, cap), out_shape=...  93 us

profile of v3, /device:TPU:1, one launch (start us, length us, event | category | flops | bytes accessed | tf_op | source)
XLA Modules:
  0.0 94.7 jit_solution(15019724485174187758)
XLA Ops:
  0.0 93.0 %layer.1 = bf16[256,512]{1,0:T(8,128)(2,1)} custom-call(bf16[256,512]{1,0:T(8,128)(2,1)} %res_h.1, bf16[256,128]{1,0:T(8,128)(2,1)} %ci_h.1, bf16[256,128]{1,0:T(8,128)(2,1)} %og_h.1, bf16[256,128]{1,0:T(8,128)(2,1)} %ig_h.1, s32[1,256]{1,0:T(1,128)} %bitcast.9, f32[3,128]{1,0:T(4,128)} %taps_h.1, f32[1,512]{1,0:T(1,128)} %bitcast.5, bf16[512,512]{1,0:T(8,128)(2,1)} %ow_h.1, ...), custom_call_target="tpu_custom_call" | custom-call | flops 11274289152 | bytes 11010048 | tf_op jit(solution)/shard_map/layer/pallas_call | solution.py:657
  93.0 1.7 %copy.16 = bf16[256,512]{1,0:T(8,128)(2,1)} copy(bf16[256,512]{1,0:T(8,128)(2,1)} %layer.1) | data formatting | bytes 524288

commit v4 on v3

--- a/solution.py
+++ b/solution.py
@@ -27,57 +27,63 @@
 NEAR = 3
 RINGS = ((3, 4), (5, 6), (7, 8), (9, 10), (11,))
 RING = len(RINGS)
-PIECES = ((3, 4, 5, 6), (7, 8, 9, 10), (11,), (1, 2), (0,))
+PIECES = ((3, 4), (5, 6), (7, 8, 9, 10), (11,), (1, 2), (0,))
 ORDER = (
     ("tokens", 0),
     ("own", 0),
     ("near", 0),
+    ("forward", 0),
     ("own", 1),
-    ("forward", 0),
     ("own", 2),
     ("forward", 1),
+    ("weights", 0),
+    ("rest", 0),
+    ("up", 0),
+    ("down", 0),
+    ("start", 0),
     ("forward", 2),
     ("own", 3),
-    ("weights", 0),
-    ("rest", 0),
     ("rest", 1),
-    ("up", 0),
+    ("up", 1),
+    ("down", 1),
+    ("start", 1),
     ("forward", 3),
-    ("down", 0),
     ("own", 4),
-    ("start", 0),
+    ("add", 0),
+    ("up", 5),
+    ("down", 5),
+    ("add", 1),
+    ("rest", 2),
+    ("rest", 3),
+    ("up", 2),
+    ("forward", 4),
+    ("down", 2),
+    ("start", 2),
+    ("back", 0),
+    ("back", 1),
+    ("rest", 4),
+    ("up", 3),
+    ("add", 2),
+    ("down", 3),
+    ("start", 3),
+    ("start", 5),
     ("up", 4),
     ("down", 4),
-    ("rest", 2),
-    ("rest", 3),
-    ("up", 1),
-    ("forward", 4),
-    ("down", 1),
-    ("add", 0),
-    ("start", 1),
-    ("up", 3),
-    ("down", 3),
-    ("back", 0),
-    ("rest", 4),
-    ("up", 2),
-    ("add", 1),
-    ("down", 2),
-    ("start", 2),
+    ("back", 2),
+    ("add", 3),
     ("start", 4),
-    ("back", 1),
-    ("add", 2),
-    ("start", 3),
+    ("add", 5),
+    ("back", 3),
+    ("combine", 0),
+    ("combine", 1),
     ("add", 4),
-    ("back", 2),
-    ("combine", 0),
-    ("add", 3),
+    ("back", 5),
     ("back", 4),
-    ("back", 3),
-    ("combine", 1),
     ("combine", 2),
+    ("combine", 3),
+    ("combine", 5),
+    ("combine", 4),
     ("gone", 0),
-    ("combine", 4),
-    ("combine", 3),
 )
 MESH = pl.DeviceIdType.MESH
 F32 = jnp.float32
@@ -173,10 +179,8 @@
     right = lax.rem(tp + 1, ntp)
     opposite = lax.rem(tp + 2, ntp)
 
-    def at_sp(dz, dx, core):
-        return (
-            lax.rem(zpos + (dz + nz), nz) * NX + lax.rem(xpos + dx, NX)
-        ) * CORES + core
+    def along_z(dz):
+        return lax.rem(zpos + (dz + nz), nz) * peers + mine
 
     def signal(sem, to):
         pl.semaphore_signal(sem, inc=1, device_id=to, device_id_type=MESH)
@@ -186,12 +190,11 @@
         signal(barrier, (sp, lax.rem(tp + d, ntp)))
     for d in (1, nsp - 1):
         signal(barrier, (lax.rem(sp + d, nsp), tp))
-    for d in range(1, NX):
-        signal(barrier, (at_sp(0, d, cpos), tp))
+    for d in range(1, peers):
+        signal(barrier, (zpos * peers + lax.rem(mine + d, peers), tp))
     for d in (1, -1, 2, -2):
-        signal(barrier, (at_sp(d, 0, cpos), tp))
-    signal(barrier, (at_sp(0, 0, 1 - cpos), tp))
-    greeted = ntp - 1 + 2 + NX - 1 + 4 + 1
+        signal(barrier, (along_z(d), tp))
+    greeted = ntp - 1 + 2 + peers - 1 + 4
 
     pairs = (
         (rt_h, rt),
@@ -215,8 +218,61 @@
     for load in loads:
         load.start()
 
-    for i in range(3):
+    for i in (1, 3, 4, 5, 6, 7):
         loads[i].wait()
+    docs = jnp.transpose(jnp.broadcast_to(doc[...].astype(F32), (8, tokens)))[:, 0:1]
+    value = (ig[...].astype(F32) * ci[...].astype(F32)).astype(BF16).astype(F32)
+    joined[8:, :] = value
+    docj[8:, :] = jnp.broadcast_to(docs, (tokens, channels))
+    halo_out[0:8, :] = value[tokens - 8 :, :]
+    halo_out[8:16, :] = docj[tokens : tokens + 8, :]
+
+    def convolve(lo, hi):
+        docs_now = docj[8 + lo : 8 + hi, :]
+        same_one = (docj[7 + lo : 7 + hi, :] == docs_now).astype(F32)
+        same_two = (docj[6 + lo : 6 + hi, :] == docs_now).astype(F32)
+        conv_sum = (
+            taps[2:3, :] * joined[8 + lo : 8 + hi, :]
+            + taps[1:2, :] * joined[7 + lo : 7 + hi, :] * same_one
+            + taps[0:1, :] * joined[6 + lo : 6 + hi, :] * same_two
+        )
+        mix[tp, lo:hi, :] = (og[lo:hi, :].astype(F32) * conv_sum).astype(BF16)
+
+    def to_tp(ref, send, recv):
+        for d in (2, 1, ntp - 1):
+            pltpu.make_async_remote_copy(
+                src_ref=ref,
+                dst_ref=ref,
+                send_sem=send,
+                recv_sem=recv,
+                device_id=(sp, lax.rem(tp + d, ntp)),
+                device_id_type=MESH,
+            ).start()
+
+    def got(ref, sem):
+        with jax.named_scope("wait"):
+            pltpu.make_async_copy(ref, ref, sem).wait()
+
+    edge = 16
+    convolve(edge, tokens)
+    with jax.named_scope("barrier"):
+        pl.semaphore_wait(barrier, greeted)
+    halo = pltpu.make_async_remote_copy(
+        src_ref=halo_out,
+        dst_ref=halo_in,
+        send_sem=halo_sem.at[0],
+        recv_sem=halo_sem.at[1],
+        device_id=(lax.rem(sp + 1, nsp), tp),
+        device_id_type=MESH,
+    )
+    halo.start()
+    for d in (2, -2):
+        signal(round_sem.at[0], (along_z(d), tp))
+    to_tp(mix.at[tp, pl.ds(edge, tokens - edge)], mix_s.at[0], mix_r.at[0])
+    to_tp(gains.at[tp], mix_s.at[1], mix_r.at[1])
+
+    loads[0].wait()
+    loads[2].wait()
     experts_iota = lax.broadcasted_iota(jnp.int32, (nsp, tokens), 0)
     first = (experts_iota == rt[0:1, :]).astype(F32)
     second = (experts_iota == rt[1:2, :]).astype(F32)
@@ -234,58 +290,6 @@
     rows8[5:8, :] = jnp.zeros((3, tokens), F32)
     cols8[...] = jnp.transpose(rows8[...])
 
-    for i in range(3, 8):
-        loads[i].wait()
-    value = (ig[...].astype(F32) * ci[...].astype(F32)).astype(BF16).astype(F32)
-    joined[8:, :] = value
-    docj[8:, :] = jnp.broadcast_to(cols8[:, 0:1], (tokens, channels))
-    halo_out[0:8, :] = value[tokens - 8 :, :]
-    halo_out[8:16, :] = jnp.broadcast_to(cols8[tokens - 8 :, 0:1], (8, channels))
-
-    def convolve(lo, hi):
-        docs_now = docj[8 + lo : 8 + hi, :]
-        same_one = (docj[7 + lo : 7 + hi, :] == docs_now).astype(F32)
-        same_two = (docj[6 + lo : 6 + hi, :] == docs_now).astype(F32)
-        conv_sum = (
-            taps[2:3, :] * joined[8 + lo : 8 + hi, :]
-            + taps[1:2, :] * joined[7 + lo : 7 + hi, :] * same_one
-            + taps[0:1, :] * joined[6 + lo : 6 + hi, :] * same_two
-        )
-        mix[tp, lo:hi, :] = (og[lo:hi, :].astype(F32) * conv_sum).astype(BF16)
-
-    def to_tp(ref, send, recv):
-        for d in (2, 1, ntp - 1):
-            pltpu.make_async_remote_copy(
-                src_ref=ref,
-                dst_ref=ref,
-                send_sem=send,
-                recv_sem=recv,
-                device_id=(sp, lax.rem(tp + d, ntp)),
-                device_id_type=MESH,
-            ).start()
-
-    def got(ref, sem):
-        with jax.named_scope("wait"):
-            pltpu.make_async_copy(ref, ref, sem).wait()
-
-    edge = 16
-    convolve(edge, tokens)
-    with jax.named_scope("barrier"):
-        pl.semaphore_wait(barrier, greeted)
-    halo = pltpu.make_async_remote_copy(
-        src_ref=halo_out,
-        dst_ref=halo_in,
-        send_sem=halo_sem.at[0],
-        recv_sem=halo_sem.at[1],
-        device_id=(lax.rem(sp + 1, nsp), tp),
-        device_id_type=MESH,
-    )
-    halo.start()
-    for d in (2, -2):
-        signal(round_sem.at[0], (at_sp(d, 0, cpos), tp))
-    to_tp(mix.at[tp, pl.ds(edge, tokens - edge)], mix_s.at[0], mix_r.at[0])
-    to_tp(gains.at[tp], mix_s.at[1], mix_r.at[1])
-
     def slots_of(r, shape, dim):
         dz, skip, _ = REGIONS[r]
         line = lax.broadcasted_iota(jnp.int32, shape, dim)
@@ -305,16 +309,14 @@
     convolve(0, edge)
     to_tp(mix.at[tp, pl.ds(0, edge)], mix_s.at[0], mix_r.at[0])
     pl.semaphore_wait(round_sem.at[0], 2)
-    for d in range(1, NX):
-        signal(round_sem.at[1], (at_sp(0, d, cpos), tp))
+    for d in range(1, peers):
+        signal(round_sem.at[1], (zpos * peers + lax.rem(mine + d, peers), tp))
 
     for i in range(8, 11):
         loads[i].wait()
     with jax.named_scope("mixwait"):
         got(mix.at[pl.ds(0, ntp - 1)], mix_r.at[0])
         got(gains.at[pl.ds(0, ntp - 1)], mix_r.at[1])
-    pl.semaphore_wait(round_sem.at[1], NX - 1)
-    signal(round_sem.at[2], (at_sp(0, 0, 1 - cpos), tp))
     pieces = jnp.concatenate([mix[q] for q in range(ntp)], axis=1).astype(F32)
     squares = jnp.sum(pieces * pieces, axis=1, keepdims=True)
     mix_scale = lax.rsqrt(squares / (channels * ntp) + EPS)
@@ -358,26 +360,38 @@
 
     ring_own(tok, 0, tokens, RING)
     with jax.named_scope("roundwait"):
-        pl.semaphore_wait(round_sem.at[2], 1)
-
-    def exchange(src, dst, send, recv, r, way):
-        dz, skip, count = REGIONS[r]
-        zz = lax.rem(zpos + (way * dz + nz), nz)
-
-        def one(i, carry):
+        pl.semaphore_wait(round_sem.at[1], peers - 1)
+
+    def exchange(src, dst, send, recv, regions, way):
+        def one(r, i):
+            dz, skip, _ = REGIONS[r]
+            zz = lax.rem(zpos + (way * dz + nz), nz)
             at = pl.ds(pl.multiple_of(base[r] + i * cap, cap), cap)
             to = lax.rem(mine + way * (i + skip) + peers, peers)
             pltpu.make_async_remote_copy(
                 src_ref=src(at),
                 dst_ref=dst(at),
                 send_sem=send,
-                recv_sem=recv,
+                recv_sem=recv(r),
                 device_id=(zz * peers + to, tp),
                 device_id_type=MESH,
             ).start()
+
+        count = REGIONS[regions[0]][2]
+
+        def turn(i, carry):
+            for r in regions:
+                one(r, i if way > 0 else count - i)
             return carry
 
-        lax.fori_loop(1 if r == 0 else 0, count, one, 0)
+        others = [r for r in regions if r != 0]
+        if way > 0:
+            for r in others:
+                one(r, 0)
+        lax.fori_loop(1, count, turn, 0)
+        if way < 0:
+            for r in others:
+                one(r, 0)
 
     ring_of = {r: g for g, regions in enumerate(RINGS) for r in regions}
 
@@ -392,37 +406,36 @@
     def rows_at(r):
         return slice(base[r], base[r] + sizes[r])
 
-    for r in range(NEAR, len(REGIONS)):
-        outgo[rows_at(r), :] = jnp.dot(
-            perm[rows_at(r), :], gained, preferred_element_type=F32
-        ).astype(BF16)
+    for g, regions in enumerate(RINGS):
+        for r in regions:
+            outgo[rows_at(r), :] = jnp.dot(
+                perm[rows_at(r), :], gained, preferred_element_type=F32
+            ).astype(BF16)
         exchange(
             lambda at: outgo.at[at],
             lambda at: xin.at[tp, at],
             disp_s.at[0],
-            disp_r.at[ring_of[r]],
-            r,
+            lambda r: disp_r.at[ring_of[r]],
+            regions,
             1,
         )
 
     def near():
         ring_rest(tok, 0, tokens, RING)
-        for r in range(NEAR):
-            for q in range(ntp):
+        for q in range(ntp):
+            for r in range(NEAR):
                 outrow[q, rows_at(r), :] = jnp.dot(
                     perm[rows_at(r), :], tok[q], preferred_element_type=F32
                 ).astype(BF16)
-            if r == 0:
-                for q in range(ntp):
-                    xin[q, 0:cap, :] = outrow[q, 0:cap, :]
-            exchange(
-                lambda at: outrow.at[:, at],
-                lambda at: xin.at[:, at],
-                disp_s.at[1],
-                disp_r.at[RING + min(r, 1)],
-                r,
-                1,
-            )
+            xin[q, 0:cap, :] = outrow[q, 0:cap, :]
+        exchange(
+            lambda at: outrow.at[:, at],
+            lambda at: xin.at[:, at],
+            disp_s.at[1],
+            lambda r: disp_r.at[RING + min(r, 1)],
+            tuple(range(NEAR)),
+            1,
+        )
 
     def span(k):
         return extent(PIECES[k])
@@ -446,7 +459,7 @@
     tile = 128
     wide = 256
 
-    def experts_up(start, rows):
+    def experts_scale(start, rows):
         total = jnp.zeros((rows, tile), F32)
         for q in range(ntp):
             weight = 1.0 / (gains[q] * gains[q])
@@ -457,6 +470,7 @@
         scale = lax.rsqrt(jnp.sum(total, axis=1, keepdims=True) / width + EPS)
         scl[0:rows, :] = jnp.broadcast_to(scale, (rows, tile))
 
+    def experts_up(start, rows):
         def up_tile(n, carry):
             at = pl.ds(pl.multiple_of(n * tile, tile), tile)
             x = jnp.concatenate([xin[q, start : start + rows] for q in range(ntp)], axis=1)
@@ -511,17 +525,16 @@
         ret[whole, :] = (
             part[tp, whole, :].astype(F32) + fl[whole, :].astype(F32) + fr[whole, :].astype(F32)
         ).astype(BF16)
-        for r in PIECES[k]:
-            if r == 0:
-                ret_in[0:cap, :] = ret[0:cap, :]
-            exchange(
-                lambda at: ret.at[at],
-                lambda at: ret_in.at[at],
-                ret_s.at[0],
-                ret_r.at[k],
-                r,
-                -1,
-            )
+        if 0 in PIECES[k]:
+            ret_in[0:cap, :] = ret[0:cap, :]
+        exchange(
+            lambda at: ret.at[at],
+            lambda at: ret_in.at[at],
+            ret_s.at[0],
+            lambda r: ret_r.at[k],
+            PIECES[k],
+            -1,
+        )
 
     def combine(k):
         got(ret_in.at[crossed(PIECES[k])], ret_r.at[k])
@@ -554,7 +567,7 @@
         "own": own,
         "forward": forward,
         "rest": rest,
-        "up": lambda k: (arrived(k), experts_up(*span(k))),
+        "up": lambda k: (arrived(k), experts_scale(*span(k)), experts_up(*span(k))),
         "down": lambda k: experts_down(*span(k)),
         "add": reduce_add,
         "back": give_back,
@@ -652,7 +665,7 @@
         dma((3, len(PIECES))),
         dma((1,)),
         dma((len(PIECES),)),
-        pltpu.SemaphoreType.REGULAR((3,)),
+        pltpu.SemaphoreType.REGULAR((2,)),
     ]
     return pl.pallas_call(
         functools.partial(layer_kernel, nsp, ntp, cap),

time: 94.8 us -> 93.3 us (0.984)
  Pallas kernels: 93 us -> 91.6 us
    pallas_call x1, Pallas kernels: 93 us -> 91.6 us  [per_device(): pl.pallas_call(functools.partial(layer_kernel, nsp, ntp, cap), out_shape=...]
where the time goes in v4:
time: 93.3 us; the launch traced here: 93.2 us
  Pallas kernels  91.6 us (98%)
  local copies, waits for them, and re-layouts  1.67 us (2%)
    pallas_call x1, Pallas kernels, per_device(): pl.pallas_call(functools.partial(layer_kernel, nsp, ntp, cap), out_shape=...  91.6 us

profile of v4, /device:TPU:1, one launch (start us, length us, event | category | flops | bytes accessed | tf_op | source)
XLA Modules:
  0.0 93.2 jit_solution(14025916257266351381)
XLA Ops:
  0.0 91.6 %layer.1 = bf16[256,512]{1,0:T(8,128)(2,1)} custom-call(bf16[256,512]{1,0:T(8,128)(2,1)} %res_h.1, bf16[256,128]{1,0:T(8,128)(2,1)} %ci_h.1, bf16[256,128]{1,0:T(8,128)(2,1)} %og_h.1, bf16[256,128]{1,0:T(8,128)(2,1)} %ig_h.1, s32[1,256]{1,0:T(1,128)} %bitcast.9, f32[3,128]{1,0:T(4,128)} %taps_h.1, f32[1,512]{1,0:T(1,128)} %bitcast.5, bf16[512,512]{1,0:T(8,128)(2,1)} %ow_h.1, ...), custom_call_target="tpu_custom_call" | custom-call | flops 11274289152 | bytes 11010048 | tf_op jit(solution)/shard_map/layer/pallas_call | solution.py:670
  91.6 1.7 %copy.16 = bf16[256,512]{1,0:T(8,128)(2,1)} copy(bf16[256,512]{1,0:T(8,128)(2,1)} %layer.1) | data formatting | bytes 524288
